TPU v7x, 32 devices: a whole 2x2x4 slice. The times are simulated.
32 devices in a mesh: ep: 8 (over z, y), tp: 4 (over x, core).
Axes of the slice: x: 2, y: 2, z: 4, core: 2. Of those that a mesh axis runs over, the one named last changes fastest.
Arguments:
- sequence_entry_features: bfloat16 [12288, 4096], P('ep', 'tp'), may hold values from -6 to 6
- sequence_exit_gating: bfloat16 [12288, 4096], P('ep', 'tp'), may hold values from -6 to 6
- memory_insert_clusters: bfloat16 [12288, 1024], P('ep', 'tp'), may hold values from -6 to 6
- memory_query_clusters: bfloat16 [12288, 1024], P('ep', 'tp'), may hold values from -6 to 6
- interval_presoftplus: bfloat16 [12288, 64], P('ep', 'tp'), may hold values from -4 to 4
- entry_filter_taps: bfloat16 [4, 4096], P(None, 'tp'), may hold values from -3 to 3
- insert_filter_taps: bfloat16 [4, 1024], P(None, 'tp'), may hold values from -3 to 3
- query_filter_taps: bfloat16 [4, 1024], P(None, 'tp'), may hold values from -3 to 3
- interval_offset: float32 [64], P('tp'), may hold values from -6 to -1
- head_fading_exponent: float32 [64], P('tp'), may hold values from -8 to -1
- skip_connection_factor: float32 [64], P('tp'), may hold values from 0.1 to 1.9
- spike_fading_exponent: float32 [12288, 64], P('ep', 'tp'), may hold values from -1 to 0
- cluster_scaling_vector: float32 [4096], P('tp'), may hold values from 0.1 to 1.9
- sequence_exit_projection: bfloat16 [4096, 2048], P('tp'), may hold values from -0.09375 to 0.09375
- specialist_sample_slice: bfloat16 [4096, 2048], P(('ep', 'tp')), may hold values from -6 to 6
- specialist_scaling_vector: float32 [2048], replicated, may hold values from 0.1 to 1.9
- chosen_specialists: int32 [4096, 4], P(('ep', 'tp')), may hold values from 0 to 7, all different within a row; in each aligned block of 128 rows (0 to 127, 128 to 255, ...) at most 80 rows name the same one
- dispatcher_affinity_matrix: float32 [4096, 4], P(('ep', 'tp')), may hold values from -4 to 4
- gating_projection: bfloat16 [8, 2048, 2048], P('ep', None, 'tp'), may hold values from -0.5 to 0.5
- expand_projection: bfloat16 [8, 2048, 2048], P('ep', None, 'tp'), may hold values from -0.5 to 0.5
- shrink_projection: bfloat16 [8, 2048, 2048], P('ep', 'tp'), may hold values from -0.03125 to 0.03125
Outputs:
- mixed: bfloat16 [12288, 2048], P(('ep', 'tp'))
- moe_out: bfloat16 [4096, 2048], P(('ep', 'tp'))
Inputs may be any that keep to these rules, and one draw needn't show every extreme that they name: `chosen_specialists`: in each aligned block of 128 rows (the rows of one device) no expert is named by more than 80 rows, a bound that some block reaches; the 4 experts of a row differ.
All inputs are finite; a program needn't handle non-finite values.
Results may differ from a plain program's by a relative error of at most 0.015.
Values may be sent and summed in bfloat16 or wider, within the bound.
A program may use at most 192 MiB of HBM per device.

v0:
```python
import functools
import jax
import jax.numpy as jnp
from jax import lax
from jax.experimental import pallas as pl
from jax.experimental.pallas import tpu as pltpu
from jax.sharding import PartitionSpec as P

HEAD = 64
STATE = 128
SPAN = 128
RIM = 8

norm_eps = 1e-05
clamp_top = 7.0
sigmoid_sharp = 1.702
highest = lax.Precision.HIGHEST


def passed_along(block, axis, distance):
    devices = range(lax.axis_size(axis))
    route = [(i - distance, i) for i in devices if i - distance in devices]
    return lax.ppermute(block, axis, route)


def conv_block(buf, first, value_ref, rim_ref, taps_ref):
    @pl.when(first)
    def _():
        buf[0:RIM, :] = rim_ref[...].astype(jnp.float32)

    @pl.when(jnp.logical_not(first))
    def _():
        buf[0:RIM, :] = buf[SPAN : SPAN + RIM, :]

    buf[RIM : RIM + SPAN, :] = value_ref[...].astype(jnp.float32)
    taps = taps_ref[...].astype(jnp.float32)
    count = taps.shape[0]
    total = buf[RIM : RIM + SPAN, :] * taps[count - 1 : count]
    for j in range(count - 1):
        start = RIM - (count - 1) + j
        total = total + buf[start : start + SPAN, :] * taps[j : j + 1]
    return total * jax.nn.sigmoid(total)


def spread(cols, h, width):
    return jnp.broadcast_to(cols[:, h : h + 1], (SPAN, width))


def state_kernel(per_group, groups, x_ref, xr_ref, xt_ref, b_ref, br_ref, bt_ref, lw_ref, end_ref,
                 state_ref, xbuf, bbuf):
    first = pl.program_id(0) == 0
    x = conv_block(xbuf, first, x_ref, xr_ref, xt_ref)
    b = conv_block(bbuf, first, b_ref, br_ref, bt_ref)

    @pl.when(first)
    def _():
        state_ref[...] = jnp.zeros_like(state_ref)

    lw = lw_ref[...]
    low = lax.broadcasted_iota(jnp.int32, (SPAN, 2 * HEAD), 1) < HEAD
    for g in range(groups):
        bt = b[:, g * STATE : (g + 1) * STATE].T.astype(jnp.bfloat16)
        for pair in range(per_group // 2):
            h = g * per_group + 2 * pair
            cols = slice(h * HEAD, (h + 2) * HEAD)
            factor = jnp.exp(jnp.where(low, spread(lw, h, 2 * HEAD), spread(lw, h + 1, 2 * HEAD)))
            xw = (x[:, cols] * factor).astype(jnp.bfloat16)
            added = jnp.dot(bt, xw, preferred_element_type=jnp.float32)
            state_ref[:, cols] = state_ref[:, cols] * end_ref[0, :, cols] + added


def output_kernel(per_group, groups, x_ref, xr_ref, xt_ref, b_ref, br_ref, bt_ref, c_ref, cr_ref,
                  ct_ref, z_ref, lw_ref, cum_ref, row_ref, end_ref, enter_ref, skip_ref, scale_ref,
                  out_ref, xbuf, bbuf, cbuf, state, ybuf):
    first = pl.program_id(0) == 0
    x = conv_block(xbuf, first, x_ref, xr_ref, xt_ref)
    b = conv_block(bbuf, first, b_ref, br_ref, bt_ref)
    c = conv_block(cbuf, first, c_ref, cr_ref, ct_ref)

    @pl.when(first)
    def _():
        state[...] = enter_ref[...]

    lw = lw_ref[...]
    cum = cum_ref[...]
    low = lax.broadcasted_iota(jnp.int32, (SPAN, 2 * HEAD), 1) < HEAD
    causal = lax.broadcasted_iota(jnp.int32, (SPAN, SPAN), 0) >= lax.broadcasted_iota(
        jnp.int32, (SPAN, SPAN), 1
    )
    group_cols = per_group * HEAD
    for g in range(groups):
        bg = b[:, g * STATE : (g + 1) * STATE]
        bt = bg.T.astype(jnp.bfloat16)
        cg = c[:, g * STATE : (g + 1) * STATE].astype(jnp.bfloat16)
        scores = jnp.dot(cg, bt, preferred_element_type=jnp.float32)
        squares = jnp.zeros((SPAN, 2 * HEAD), jnp.float32)
        for pair in range(per_group // 2):
            h = g * per_group + 2 * pair
            cols = slice(h * HEAD, (h + 2) * HEAD)
            xp = x[:, cols]
            cum_0, cum_1 = spread(cum, h, SPAN), spread(cum, h + 1, SPAN)
            m_0 = scores * jnp.exp(jnp.where(causal, cum_0 + row_ref[0, h : h + 1, :], -jnp.inf))
            m_1 = scores * jnp.exp(jnp.where(causal, cum_1 + row_ref[0, h + 1 : h + 2, :], -jnp.inf))
            mixing = jnp.concatenate([m_0.astype(jnp.bfloat16), m_1.astype(jnp.bfloat16)], axis=1)
            x_0 = jnp.where(low, xp, 0.0).astype(jnp.bfloat16)
            x_1 = jnp.where(low, 0.0, xp).astype(jnp.bfloat16)
            y = jnp.dot(
                mixing, jnp.concatenate([x_0, x_1], axis=0), preferred_element_type=jnp.float32
            )
            before = state[:, cols]
            carried = jnp.dot(cg, before.astype(jnp.bfloat16), preferred_element_type=jnp.float32)
            y = y + carried * jnp.exp(jnp.where(low, cum_0, cum_1)) + xp * skip_ref[:, cols]
            factor = jnp.exp(jnp.where(low, spread(lw, h, 2 * HEAD), spread(lw, h + 1, 2 * HEAD)))
            xw = (xp * factor).astype(jnp.bfloat16)
            added = jnp.dot(bt, xw, preferred_element_type=jnp.float32)
            state[:, cols] = before * end_ref[0, :, cols] + added
            gate = z_ref[:, cols].astype(jnp.float32)
            gated = y * (gate * jax.nn.sigmoid(gate))
            squares = squares + gated * gated
            ybuf[:, cols] = gated
        mean = jnp.sum(squares, axis=1, keepdims=True) / group_cols
        inverse = lax.rsqrt(mean + norm_eps)
        cols = slice(g * group_cols, (g + 1) * group_cols)
        out_ref[:, cols] = (ybuf[:, cols] * inverse * scale_ref[:, cols]).astype(jnp.bfloat16)


def entering_state(own_state, own_decay):
    size, mine = (lax.axis_size("ep"), lax.axis_index("ep"))
    rows = own_state.shape[0]
    total = own_state
    decay = own_decay

    def joined():
        return jnp.concatenate(
            [total, jnp.broadcast_to(decay, (RIM, decay.shape[1]))], axis=0
        ).astype(jnp.bfloat16)

    distance = 1
    while distance < size:
        came = passed_along(joined(), "ep", distance)
        there = mine >= distance
        earlier = came[:rows].astype(jnp.float32)
        earlier_decay = jnp.where(there, came[rows : rows + 1].astype(jnp.float32), 1.0)
        total = earlier * decay + total
        decay = earlier_decay * decay
        distance *= 2
    return passed_along(total.astype(jnp.bfloat16), "ep", 1).astype(jnp.float32)


def mixer_half(
    sequence_entry_features,
    sequence_exit_gating,
    memory_insert_clusters,
    memory_query_clusters,
    interval_presoftplus,
    entry_filter_taps,
    insert_filter_taps,
    query_filter_taps,
    interval_offset,
    head_fading_exponent,
    skip_connection_factor,
    spike_fading_exponent,
    cluster_scaling_vector,
    sequence_exit_projection,
):
    tok_rows = sequence_entry_features.shape[0]
    local_heads = interval_offset.shape[0]
    local_groups = memory_insert_clusters.shape[1] // STATE
    per_group = local_heads // local_groups
    inner_cols = sequence_entry_features.shape[1]
    state_cols = memory_insert_clusters.shape[1]
    last_rows = jnp.concatenate(
        [
            sequence_entry_features[tok_rows - RIM :],
            memory_insert_clusters[tok_rows - RIM :],
            memory_query_clusters[tok_rows - RIM :],
        ],
        axis=1,
    )
    rims = passed_along(last_rows, "ep", 1)
    rim_x = rims[:, :inner_cols]
    rim_b = rims[:, inner_cols : inner_cols + state_cols]
    rim_c = rims[:, inner_cols + state_cols :]
    blocks = tok_rows // SPAN
    interval = jax.nn.softplus(interval_presoftplus.astype(jnp.float32) + interval_offset)
    fading = spike_fading_exponent - jnp.exp(head_fading_exponent) * interval
    lower = jnp.tril(jnp.ones((SPAN, SPAN), jnp.float32))
    cumulative = jnp.einsum(
        "ts,csh->cth", lower, fading.reshape(blocks, SPAN, local_heads), precision=highest
    )
    log_step = jnp.log(interval).reshape(blocks, SPAN, local_heads)
    block_end = cumulative[:, -1:]
    key_log = (log_step - cumulative + block_end).reshape(tok_rows, local_heads)
    row_log = jnp.swapaxes(log_step - cumulative, 1, 2)
    end_factor = jnp.repeat(jnp.exp(block_end), HEAD, axis=2)
    own_decay = jnp.repeat(jnp.exp(jnp.sum(block_end, axis=0)), HEAD, axis=1)
    cumulative = cumulative.reshape(tok_rows, local_heads)

    def rows_of(width):
        return pl.BlockSpec((SPAN, width), lambda i: (i, 0))

    def fixed(shape):
        return pl.BlockSpec(shape, lambda i: (0, 0))

    def block_of(rows, width):
        return pl.BlockSpec((1, rows, width), lambda i: (i, 0, 0))

    def cost(dots):
        return pl.CostEstimate(
            flops=dots * tok_rows * inner_cols * STATE * 8,
            bytes_accessed=dots * tok_rows * inner_cols * 8,
            transcendentals=0,
        )

    taps = entry_filter_taps.shape[0]
    x_specs = [rows_of(inner_cols), fixed((RIM, inner_cols)), fixed((taps, inner_cols))]
    s_specs = [rows_of(state_cols), fixed((RIM, state_cols)), fixed((taps, state_cols))]
    x_args = (sequence_entry_features, rim_x, entry_filter_taps)
    b_args = (memory_insert_clusters, rim_b, insert_filter_taps)
    c_args = (memory_query_clusters, rim_c, query_filter_taps)
    own_state = pl.pallas_call(
        functools.partial(state_kernel, per_group, local_groups),
        grid=(blocks,),
        in_specs=x_specs + s_specs + [rows_of(local_heads), block_of(1, inner_cols)],
        out_specs=fixed((STATE, inner_cols)),
        out_shape=jax.ShapeDtypeStruct((STATE, inner_cols), jnp.float32),
        scratch_shapes=[
            pltpu.VMEM((SPAN + RIM, inner_cols), jnp.float32),
            pltpu.VMEM((SPAN + RIM, state_cols), jnp.float32),
        ],
        cost_estimate=cost(1),
        name="own_state",
    )(*x_args, *b_args, key_log, end_factor)
    entering = entering_state(own_state, own_decay)
    normed = pl.pallas_call(
        functools.partial(output_kernel, per_group, local_groups),
        grid=(blocks,),
        in_specs=x_specs + s_specs + s_specs + [
            rows_of(inner_cols),
            rows_of(local_heads),
            rows_of(local_heads),
            block_of(local_heads, SPAN),
            block_of(1, inner_cols),
            fixed((STATE, inner_cols)),
            fixed((1, inner_cols)),
            fixed((1, inner_cols)),
        ],
        out_specs=rows_of(inner_cols),
        out_shape=jax.ShapeDtypeStruct((tok_rows, inner_cols), jnp.bfloat16),
        scratch_shapes=[
            pltpu.VMEM((SPAN + RIM, inner_cols), jnp.float32),
            pltpu.VMEM((SPAN + RIM, state_cols), jnp.float32),
            pltpu.VMEM((SPAN + RIM, state_cols), jnp.float32),
            pltpu.VMEM((STATE, inner_cols), jnp.float32),
            pltpu.VMEM((SPAN, inner_cols), jnp.float32),
        ],
        cost_estimate=cost(3),
        name="mixer_output",
    )(
        *x_args, *b_args, *c_args, sequence_exit_gating, key_log, cumulative, row_log, end_factor,
        entering, jnp.repeat(skip_connection_factor, HEAD)[None], cluster_scaling_vector[None],
    )
    return lax.psum_scatter(
        jnp.dot(normed, sequence_exit_projection, preferred_element_type=jnp.float32).astype(
            jnp.bfloat16
        ),
        "tp",
        scatter_dimension=0,
        tiled=True,
    )


def experts_half(
    specialist_sample_slice,
    specialist_scaling_vector,
    chosen_specialists,
    dispatcher_affinity_matrix,
    gating_projection,
    expand_projection,
    shrink_projection,
):
    tok_rows = specialist_sample_slice.shape[0]
    feature_count = specialist_sample_slice.shape[1]
    top_count = chosen_specialists.shape[1]
    experts = lax.axis_size("ep")
    groups_tp = lax.axis_size("tp")
    capacity = tok_rows * top_count * 5 // (4 * experts)
    as_float = specialist_sample_slice.astype(jnp.float32)
    centred = as_float - jnp.mean(as_float, axis=1, keepdims=True)
    normed = (
        centred
        * lax.rsqrt(jnp.mean(centred * centred, axis=1, keepdims=True) + norm_eps)
        * specialist_scaling_vector
    ).astype(jnp.bfloat16)
    route_weight = jnp.exp(dispatcher_affinity_matrix) / jnp.sum(
        jnp.exp(dispatcher_affinity_matrix), axis=1, keepdims=True
    )
    flat_routes = chosen_specialists.reshape(-1)
    onehot = (flat_routes[:, None] == jnp.arange(experts, dtype=jnp.int32)[None, :]).astype(
        jnp.int32
    )
    position = jnp.sum(onehot * (jnp.cumsum(onehot, axis=0) - 1), axis=1)
    target = flat_routes * capacity + position
    token_ids = jnp.arange(tok_rows * top_count, dtype=jnp.int32) // top_count
    source_table = jnp.full((experts * capacity,), tok_rows, jnp.int32).at[target].set(token_ids)
    padded = jnp.concatenate([normed, jnp.zeros((1, feature_count), jnp.bfloat16)], axis=0)
    outgoing = padded[source_table].reshape(experts, capacity, feature_count)
    arrived = lax.all_to_all(outgoing, "ep", split_axis=0, concat_axis=0, tiled=True)
    shard_rows = lax.all_gather(arrived, "tp", axis=0, tiled=True)
    rows_in = shard_rows.reshape(-1, feature_count)
    gate_h = jnp.dot(rows_in, gating_projection[0], preferred_element_type=jnp.float32)
    up_h = jnp.dot(rows_in, expand_projection[0], preferred_element_type=jnp.float32)
    clipped = jnp.minimum(gate_h, clamp_top)
    hidden_act = (
        (
            clipped
            * jax.nn.sigmoid(sigmoid_sharp * clipped)
            * (jnp.clip(up_h, -clamp_top, clamp_top) + 1.0)
        )
        .astype(jnp.bfloat16)
        .reshape(shard_rows.shape[0], capacity, -1)
    )
    hidden_act = hidden_act.reshape(groups_tp * experts * capacity, -1)
    summed = lax.psum_scatter(
        jnp.dot(hidden_act, shrink_projection[0], preferred_element_type=jnp.float32).astype(
            jnp.bfloat16
        ),
        "tp",
        scatter_dimension=0,
        tiled=True,
    )
    returned = lax.all_to_all(
        summed.reshape(experts, capacity, feature_count),
        "ep",
        split_axis=0,
        concat_axis=0,
        tiled=True,
    )
    slot_out = returned.reshape(experts * capacity, feature_count)[target].reshape(
        tok_rows, top_count, feature_count
    )
    combined = jnp.einsum("tk,tkd->td", route_weight, slot_out.astype(jnp.float32))
    return combined.astype(jnp.bfloat16)


def body(
    sequence_entry_features,
    sequence_exit_gating,
    memory_insert_clusters,
    memory_query_clusters,
    interval_presoftplus,
    entry_filter_taps,
    insert_filter_taps,
    query_filter_taps,
    interval_offset,
    head_fading_exponent,
    skip_connection_factor,
    spike_fading_exponent,
    cluster_scaling_vector,
    sequence_exit_projection,
    specialist_sample_slice,
    specialist_scaling_vector,
    chosen_specialists,
    dispatcher_affinity_matrix,
    gating_projection,
    expand_projection,
    shrink_projection,
):
    mixed = mixer_half(
        sequence_entry_features,
        sequence_exit_gating,
        memory_insert_clusters,
        memory_query_clusters,
        interval_presoftplus,
        entry_filter_taps,
        insert_filter_taps,
        query_filter_taps,
        interval_offset,
        head_fading_exponent,
        skip_connection_factor,
        spike_fading_exponent,
        cluster_scaling_vector,
        sequence_exit_projection,
    )
    moe_out = experts_half(
        specialist_sample_slice,
        specialist_scaling_vector,
        chosen_specialists,
        dispatcher_affinity_matrix,
        gating_projection,
        expand_projection,
        shrink_projection,
    )
    return (mixed, moe_out)


def solution(mesh):
    in_specs = (
        P("ep", "tp"),
        P("ep", "tp"),
        P("ep", "tp"),
        P("ep", "tp"),
        P("ep", "tp"),
        P(None, "tp"),
        P(None, "tp"),
        P(None, "tp"),
        P("tp"),
        P("tp"),
        P("tp"),
        P("ep", "tp"),
        P("tp"),
        P("tp", None),
        P(("ep", "tp"), None),
        P(),
        P(("ep", "tp"), None),
        P(("ep", "tp"), None),
        P("ep", None, "tp"),
        P("ep", None, "tp"),
        P("ep", "tp", None),
    )
    out_specs = (P(("ep", "tp"), None), P(("ep", "tp"), None))
    return jax.shard_map(body, mesh=mesh, in_specs=in_specs, out_specs=out_specs, check_vma=False)
```

profile of v0, /device:TPU:0, one launch (start us, length us, event | category | flops | bytes accessed | tf_op | source)
XLA Modules:
  0.0 386.7 jit_solution(12623622830207606083)
XLA Ops:
  9.1 1.1 reduce-window.6
  10.8 2.4 scatter_custom_fusion
  13.3 1.2 convert_reduce_fusion
  14.5 1.3 fusion.9
  15.8 1.4 fusion.11
  17.3 4.1 %gather_fusion = bf16[640,2048]{1,0:T(8,128)(2,1)} fusion(bf16[129,2048]{1,0:T(8,128)(2,1)S(1)} %concatenate.22, s32[1024]{0:T(1024)S(1)} %pad_clamp_fusion.1), kind=kCustom, calls=%fused_computation | custom fusion | bytes 5245440 | tf_op jit(solution)/shard_map/gather | solution.py:307
  21.4 66.9 %all_to_all.10 = bf16[8,80,2048]{2,1,0:T(8,128)(2,1)} all-to-all(bf16[8,80,2048]{2,1,0:T(8,128)(2,1)} %bitcast.58), channel_id=1, replica_groups=mesh['ep'=8,'tp'=4] {'ep'}, dimensions={0} | all-to-all | bytes 5242880 | tf_op jit(solution)/shard_map/all_to_all | solution.py:308
  88.4 69.3 %all-gather.2.cloned.1.call-done = bf16[32,80,2048]{2,1,0:T(8,128)(2,1)} async-done(((bf16[8,80,2048]{2,1,0:T(8,128)(2,1)}), bf16[32,80,2048]{2,1,0:T(8,128)(2,1)}) %all-gather.2.cloned.1.call-update) | async-done | bytes 10485776 | tf_op jit(solution)/shard_map/all_gather | solution.py:309
  157.6 10.5 %convolution_clamp_fusion = f32[2560,512]{1,0:T(8,128)} fusion(bf16[2560,2048]{1,0:T(8,128)(2,1)} %bitcast.72, bf16[1,2048,512]{2,1,0:T(8,128)(2,1)} %param.40), kind=kOutput, calls=%fused_computation.5 | convolution fusion | flops 5370019840 | bytes 17825792 | tf_op jit(solution)/shard_map/dot_general | solution.py:312
  168.1 18.5 %convolution_convert_fusion = bf16[2560,2048]{1,0:T(8,128)(2,1)} fusion(f32[2560,512]{1,0:T(8,128)} %convolution_clamp_fusion, bf16[2560,2048]{1,0:T(8,128)(2,1)} %bitcast.73, bf16[1,512,2048]{2,1,0:T(8,128)(2,1)S(1)} %copy-done, bf16[1,2048,512]{2,1,0:T(8,128)(2,1)} %param.39), kind=kOutput, calls=%fused_computation.3 | convolution fusion | flops 10754457600 | bytes 30408704 | tf_op jit(solution)/shard_map/dot_general | solution.py:325
  187.3 3.6 collective-permute-start
  192.3 1.2 copy.47
  195.6 16.2 %own_state.1 = f32[128,1024]{1,0:T(8,128)} custom-call(bf16[1536,1024]{1,0:T(8,128)(2,1)} %x_ref.3, bf16[8,1024]{1,0:T(8,128)(2,1)} %slice.60.xr_ref, bf16[4,1024]{1,0:T(4,128)(2,1)} %xt_ref.3, bf16[1536,256]{1,0:T(8,128)(2,1)} %b_ref.3, bf16[8,256]{1,0:T(8,128)(2,1)} %get-tuple-element.10.br_ref, bf16[4,256]{1,0:T(4,128)(2,1)} %bt_ref.3, ...), custom_call_target="tpu_custom_call" | custom-call | flops 1610612736 | bytes 12582912 | tf_op jit(solution)/shard_map/own_state/pallas_call | solution.py:221
  211.9 1.2 convert.21
  213.1 3.4 collective-permute-start.1
  216.6 6.0 %collective-permute-done.1 = bf16[136,1024]{1,0:T(8,128)(2,1)S(1)} collective-permute-done((bf16[136,1024]{1,0:T(8,128)(2,1)S(1)}, bf16[136,1024]{1,0:T(8,128)(2,1)S(1)}, u32[]{:S(2)}, u32[]{:S(2)}) %collective-permute-start.1) | collective-permute-done | bytes 278560 | tf_op jit(solution)/shard_map/ppermute | solution.py:23
  222.6 1.1 fusion.12
  223.8 5.3 %collective-permute-start.2 = (bf16[136,1024]{1,0:T(8,128)(2,1)S(1)}, bf16[136,1024]{1,0:T(8,128)(2,1)S(1)}, u32[]{:S(2)}, u32[]{:S(2)}) collective-permute-start(bf16[136,1024]{1,0:T(8,128)(2,1)S(1)} %pad_maximum_fusion.1), channel_id=1, source_target_pairs={{0,8},{4,12},{8,16},{12,20},{16,24},{20,28},{1,9},{5,13},{9,17},{1... | collective-permute-start | bytes 835592 | tf_op jit(solution)/shard_map/ppermute | solution.py:23
  229.1 5.2 %collective-permute-done.2 = bf16[136,1024]{1,0:T(8,128)(2,1)S(1)} collective-permute-done((bf16[136,1024]{1,0:T(8,128)(2,1)S(1)}, bf16[136,1024]{1,0:T(8,128)(2,1)S(1)}, u32[]{:S(2)}, u32[]{:S(2)}) %collective-permute-start.2) | collective-permute-done | bytes 278560 | tf_op jit(solution)/shard_map/ppermute | solution.py:23
  234.3 1.2 fusion.15
  235.5 5.3 %collective-permute-start.3 = (bf16[136,1024]{1,0:T(8,128)(2,1)S(1)}, bf16[136,1024]{1,0:T(8,128)(2,1)S(1)}, u32[]{:S(2)}, u32[]{:S(2)}) collective-permute-start(bf16[136,1024]{1,0:T(8,128)(2,1)S(1)} %pad_maximum_fusion.2), channel_id=1, source_target_pairs={{0,16},{4,20},{8,24},{12,28},{1,17},{5,21},{9,25},{13,29},{2,18},{... | collective-permute-start | bytes 835592 | tf_op jit(solution)/shard_map/ppermute | solution.py:23
  240.8 4.5 %collective-permute-done.3 = bf16[136,1024]{1,0:T(8,128)(2,1)S(1)} collective-permute-done((bf16[136,1024]{1,0:T(8,128)(2,1)S(1)}, bf16[136,1024]{1,0:T(8,128)(2,1)S(1)}, u32[]{:S(2)}, u32[]{:S(2)}) %collective-permute-start.3) | collective-permute-done | bytes 278560 | tf_op jit(solution)/shard_map/ppermute | solution.py:23
  245.5 2.7 collective-permute-start.4
  248.2 1.2 copy.46
  250.1 2.0 collective-permute-done.4
  252.9 25.6 %mixer_output.1 = bf16[1536,1024]{1,0:T(8,128)(2,1)} custom-call(bf16[1536,1024]{1,0:T(8,128)(2,1)} %x_ref.3, bf16[8,1024]{1,0:T(8,128)(2,1)} %slice.60.xr_ref, bf16[4,1024]{1,0:T(4,128)(2,1)} %xt_ref.3, bf16[1536,256]{1,0:T(8,128)(2,1)} %b_ref.3, bf16[8,256]{1,0:T(8,128)(2,1)} %get-tuple-element.10.br_ref, bf16[4,256]{1,0:T(4,128)(2,1)} %bt_ref.3, ...), custom_call_target="tpu_custom_call" | custom-call | flops 4831838208 | bytes 37748736 | tf_op jit(solution)/shard_map/mixer_output/pallas_call | solution.py:235
  278.5 11.2 %convolution_convert_fusion.1 = bf16[1536,2048]{1,0:T(8,128)(2,1)} fusion(bf16[1536,1024]{1,0:T(8,128)(2,1)} %mixer_output.1, bf16[1024,2048]{1,0:T(8,128)(2,1)} %param.34), kind=kOutput, calls=%fused_computation.4 | convolution fusion | flops 6445596672 | bytes 13631488 | tf_op jit(solution)/shard_map/dot_general | solution.py:264
  289.8 16.0 %all-to-all-start.1 = ((bf16[8,80,2048]{2,1,0:T(8,128)(2,1)}), bf16[8,80,2048]{2,1,0:T(8,128)(2,1)}, u32[]{:S(2)}, u32[]{:S(2)}) async-start(bf16[8,80,2048]{2,1,0:T(8,128)(2,1)} %bitcast.59), calls=%async_computation.3 | async-start | bytes 5242880 | tf_op jit(solution)/shard_map/all_to_all | solution.py:332
  305.9 58.7 %all-to-all-done.1 = bf16[8,80,2048]{2,1,0:T(8,128)(2,1)} async-done(((bf16[8,80,2048]{2,1,0:T(8,128)(2,1)}), bf16[8,80,2048]{2,1,0:T(8,128)(2,1)}, u32[]{:S(2)}, u32[]{:S(2)}) %all-to-all-start.1) | async-done | bytes 2621472 | tf_op jit(solution)/shard_map/all_to_all | solution.py:332
  364.7 7.5 %gather_fusion.1 = bf16[512,2048]{1,0:T(8,128)(2,1)} fusion(bf16[640,2048]{1,0:T(8,128)(2,1)} %bitcast.18, s32[1024]{0:T(1024)S(1)} %pad_clamp_fusion), kind=kCustom, calls=%fused_computation.1 | custom fusion | bytes 4196352 | tf_op jit(solution)/shard_map/gather | solution.py:339
  372.2 4.1 %reshape.120 = bf16[128,4,2048]{2,1,0:T(4,128)(2,1)} reshape(bf16[512,2048]{1,0:T(8,128)(2,1)} %gather_fusion.1) | data formatting | bytes 4194304 | tf_op jit(solution)/shard_map/reshape | solution.py:339
  376.3 2.8 fusion.36
  (85 shorter events, 10.0 us)
Async XLA Ops:
  7.2 161.0 %copy-start = (bf16[1,512,2048]{2,1,0:T(8,128)(2,1)S(1)}, bf16[1,512,2048]{2,1,0:T(8,128)(2,1)}, u32[]{:S(2)}) copy-start(bf16[1,512,2048]{2,1,0:T(8,128)(2,1)} %param.41) | copy-start | bytes 6291460
  7.2 150.5 %all-gather.2.cloned.1.call-start = ((), (), s32[]{:S(2)}) async-start(), calls=%async_computation.5 | async-start | bytes 13107200 | tf_op jit(solution)/shard_map/all_gather | solution.py:309
  88.3 201.4 %reduce-scatter.5.cloned.1.call-start = ((), (), s32[]{:S(2)}) async-start(), calls=%async_computation.6 | async-start | bytes 13107200 | tf_op jit(solution)/shard_map/reduce_scatter | solution.py:324
  186.6 0.7 slice-start
  186.6 0.7 slice-start.1
  186.6 0.7 slice-start.2
  186.6 4.3 %copy-start.8 = (f32[16]{0:T(128)S(1)}, f32[16]{0:T(128)}, u32[]{:S(2)}) copy-start(f32[16]{0:T(128)} %param.30) | copy-start | bytes 196
  186.6 4.3 %copy-start.3 = (f32[1536,16]{0,1:T(8,128)S(1)}, f32[1536,16]{0,1:T(8,128)}, u32[]{:S(2)}) copy-start(f32[1536,16]{0,1:T(8,128)} %param.32) | copy-start | bytes 294916
  186.6 4.3 %copy-start.4 = (bf16[1536,16]{0,1:T(8,128)(2,1)S(1)}, bf16[1536,16]{0,1:T(8,128)(2,1)}, u32[]{:S(2)}) copy-start(bf16[1536,16]{0,1:T(8,128)(2,1)} %param.25) | copy-start | bytes 147460
  186.6 4.3 %copy-start.6 = (f32[16]{0:T(128)S(1)}, f32[16]{0:T(128)}, u32[]{:S(2)}) copy-start(f32[16]{0:T(128)} %param.29) | copy-start | bytes 196
  186.7 193.5 %reduce-scatter.3.cloned.1.call-start = ((), (), s32[]{:S(2)}) async-start(), calls=%async_computation.4 | async-start | bytes 7864320 | tf_op jit(solution)/shard_map/reduce_scatter | solution.py:263
  187.3 7.1 %collective-permute-start = (bf16[8,1536]{1,0:T(8,128)(2,1)S(1)}, bf16[8,1536]{1,0:T(8,128)(2,1)S(1)}, u32[]{:S(2)}, u32[]{:S(2)}) collective-permute-start(bf16[8,1536]{1,0:T(8,128)(2,1)S(1)} %pad_maximum_fusion.3), channel_id=1, source_target_pairs={{0,4},{4,8},{8,12},{12,16},{16,20},{20,24},{24,28},{1,5},{5,9},{9,... | collective-permute-start | bytes 73736 | tf_op jit(solution)/shard_map/ppermute | solution.py:23
  211.9 33.5 %copy-start.2 = (f32[128,1024]{1,0:T(8,128)S(1)}, f32[128,1024]{1,0:T(8,128)}, u32[]{:S(2)}) copy-start(f32[128,1024]{1,0:T(8,128)} %own_state.1) | copy-start | bytes 1572868
  211.9 37.5 %copy-start.7 = (f32[16]{0:T(128)S(1)}, f32[16]{0:T(128)}, u32[]{:S(2)}) copy-start(f32[16]{0:T(128)} %param.31) | copy-start | bytes 196
  213.1 9.4 %collective-permute-start.1 = (bf16[136,1024]{1,0:T(8,128)(2,1)S(1)}, bf16[136,1024]{1,0:T(8,128)(2,1)S(1)}, u32[]{:S(2)}, u32[]{:S(2)}) collective-permute-start(bf16[136,1024]{1,0:T(8,128)(2,1)S(1)} %pad_maximum_fusion), channel_id=1, source_target_pairs={{0,4},{4,8},{8,12},{12,16},{16,20},{20,24},{24,28},{1,5},{5,9},{9,... | collective-permute-start | bytes 835592 | tf_op jit(solution)/shard_map/ppermute | solution.py:23
  223.8 10.5 %collective-permute-start.2 = (bf16[136,1024]{1,0:T(8,128)(2,1)S(1)}, bf16[136,1024]{1,0:T(8,128)(2,1)S(1)}, u32[]{:S(2)}, u32[]{:S(2)}) collective-permute-start(bf16[136,1024]{1,0:T(8,128)(2,1)S(1)} %pad_maximum_fusion.1), channel_id=1, source_target_pairs={{0,8},{4,12},{8,16},{12,20},{16,24},{20,28},{1,9},{5,13},{9,17},{1... | collective-permute-start | bytes 835592 | tf_op jit(solution)/shard_map/ppermute | solution.py:23
  235.5 9.8 %collective-permute-start.3 = (bf16[136,1024]{1,0:T(8,128)(2,1)S(1)}, bf16[136,1024]{1,0:T(8,128)(2,1)S(1)}, u32[]{:S(2)}, u32[]{:S(2)}) collective-permute-start(bf16[136,1024]{1,0:T(8,128)(2,1)S(1)} %pad_maximum_fusion.2), channel_id=1, source_target_pairs={{0,16},{4,20},{8,24},{12,28},{1,17},{5,21},{9,25},{13,29},{2,18},{... | collective-permute-start | bytes 835592 | tf_op jit(solution)/shard_map/ppermute | solution.py:23
  245.5 6.6 %collective-permute-start.4 = (bf16[128,1024]{1,0:T(8,128)(2,1)S(1)}, bf16[128,1024]{1,0:T(8,128)(2,1)S(1)}, u32[]{:S(2)}, u32[]{:S(2)}) collective-permute-start(bf16[128,1024]{1,0:T(8,128)(2,1)S(1)} %add_convert_fusion), channel_id=1, source_target_pairs={{0,4},{4,8},{8,12},{12,16},{16,20},{20,24},{24,28},{1,5},{5,9},{9,... | collective-permute-start | bytes 786440 | tf_op jit(solution)/shard_map/ppermute | solution.py:23
  289.7 16.0 %copy-start.5 = (f32[128,4]{0,1:T(4,128)S(1)}, f32[128,4]{0,1:T(4,128)}, u32[]{:S(2)}) copy-start(f32[128,4]{0,1:T(4,128)} %param.38) | copy-start | bytes 6148
  289.8 74.9 %all-to-all-start.1 = ((bf16[8,80,2048]{2,1,0:T(8,128)(2,1)}), bf16[8,80,2048]{2,1,0:T(8,128)(2,1)}, u32[]{:S(2)}, u32[]{:S(2)}) async-start(bf16[8,80,2048]{2,1,0:T(8,128)(2,1)} %bitcast.59), calls=%async_computation.3 | async-start | bytes 5242880 | tf_op jit(solution)/shard_map/all_to_all | solution.py:332
  364.7 15.6 %copy-start.1 = (bf16[1,512,2048]{2,1,0:T(8,128)(2,1)S(1)}, bf16[1,512,2048]{2,1,0:T(8,128)(2,1)}, u32[]{:S(2)}) copy-start(bf16[1,512,2048]{2,1,0:T(8,128)(2,1)} %param.41) | copy-start | bytes 6291460
Sparse Core Ops, SparseCore 0:
  88.4 69.1 all-gather.1
  186.8 84.4 reduce-scatter.4
  289.8 69.3 reduce-scatter.2
where the time goes:
time: 388 us; the launch traced here: 387 us
  waiting for transfers between devices  146 us (38%)
  blocking collectives  66.9 us (17%)
  matrix products  43.2 us (11%)
  Pallas kernels  41.9 us (11%)
  starting transfers between devices  36.4 us (9%)
  local copies, waits for them, and re-layouts  27 us (7%)
  between operations  14.1 us (4%)
  other arithmetic  11.6 us (3%)
    all_gather x1, waiting for transfers between devices, experts_half(): shard_rows = lax.all_gather(arrived, 'tp', axis=0, tiled=True)  69.3 us
    all_to_all x1, blocking collectives, experts_half(): lax.all_to_all(outgoing, 'ep', split_axis=0, concat_axis=0, tiled=True)  66.9 us
    all_to_all x1, waiting for transfers between devices, experts_half(): lax.all_to_all(summed.reshape(experts, capacity, feature_count), 'ep', sp...  58.7 us
    pallas_call x1, Pallas kernels, mixer_half(): pl.pallas_call(functools.partial(output_kernel, per_group, local_groups),...  25.6 us
    ppermute x5, starting transfers between devices, passed_along(): return lax.ppermute(block, axis, route)  20.3 us
    dot_general x1, matrix products, experts_half(): jnp.dot(hidden_act, shrink_projection[0], preferred_element_type=jnp.floa...  18.5 us
    ppermute x5, waiting for transfers between devices, passed_along(): return lax.ppermute(block, axis, route)  17.6 us
    pallas_call x1, Pallas kernels, mixer_half(): pl.pallas_call(functools.partial(state_kernel, per_group, local_groups),...  16.2 us
  transfers between devices with their start and end apart: 9, of which 6 were waited for; matrix products, arithmetic and copies ran while one was open for 10% of the time, Pallas kernels for 11%

commit v1 on v0

--- a/solution.py
+++ b/solution.py
@@ -10,6 +10,7 @@
 STATE = 128
 SPAN = 128
 RIM = 8
+LANES = 128
 
 norm_eps = 1e-05
 clamp_top = 7.0
@@ -343,6 +344,327 @@
     return combined.astype(jnp.bfloat16)
 
 
+def routing_kernel(experts, x_ref, scale_ref, chosen_ref, score_ref, out_ref):
+    features = x_ref.shape[1]
+    rows, top_count = chosen_ref.shape
+    value = x_ref[...].astype(jnp.float32)
+    centred = value - jnp.mean(value, axis=1, keepdims=True)
+    spread_of = jnp.mean(centred * centred, axis=1, keepdims=True)
+    normed = centred * lax.rsqrt(spread_of + norm_eps) * scale_ref[...]
+    out_ref[:, :features] = normed.astype(jnp.bfloat16)
+    raised = jnp.exp(score_ref[...])
+    weight = raised / jnp.sum(raised, axis=1, keepdims=True)
+    lane = lax.broadcasted_iota(jnp.int32, (rows, LANES), 1)
+    named = lax.rem(lane, experts)
+    chosen = chosen_ref[...]
+    held = jnp.zeros((rows, LANES), jnp.float32)
+    share = jnp.zeros((rows, LANES), jnp.float32)
+    for k in range(top_count):
+        same = chosen[:, k : k + 1] == named
+        held = held + jnp.where(same, 1.0, 0.0)
+        share = share + jnp.where(same, weight[:, k : k + 1], 0.0)
+    earlier = lax.broadcasted_iota(jnp.int32, (rows, rows), 0) > lax.broadcasted_iota(
+        jnp.int32, (rows, rows), 1
+    )
+    place = jnp.dot(
+        jnp.where(earlier, 1.0, 0.0).astype(jnp.bfloat16),
+        held.astype(jnp.bfloat16),
+        preferred_element_type=jnp.float32,
+    )
+    place = jnp.where(held > 0.0, place, 255.0)
+    coarse = share.astype(jnp.bfloat16).astype(jnp.float32)
+    table = jnp.where(lane < experts, place, jnp.where(lane < 2 * experts, coarse, share - coarse))
+    out_ref[:, features:] = table.astype(jnp.bfloat16)
+
+
+def experts_kernel(
+    experts, capacity, tokens_ref, gate_ref, up_ref, down_ref, out_ref,
+    tokens, slots, own, outgoing, incoming, place, place_next, from_x, from_y,
+    to_y, came_y, to_x, came_x, keep_a, keep_b, to_z, from_z,
+    token_sem, core_send, core_recv, x_send, x_recv, y_send, y_recv,
+    a_send, a_recv, b_send, b_recv, z_send, z_recv,
+):
+    depth = experts // 2
+    steps = experts
+    ep, tp = lax.axis_index("ep"), lax.axis_index("tp")
+    z, y, x, core = ep // 2, ep % 2, tp // 2, tp % 2
+    next_ep = z * 2 + 1 - y
+    sibling = {"tp": x * 2 + 1 - core}
+    x_next = {"tp": (1 - x) * 2 + core}
+    y_next = {"ep": next_ep}
+    rows = out_ref.shape[0]
+    features = out_ref.shape[1]
+    half = features // 2
+    mesh_id = pl.DeviceIdType.MESH
+
+    def z_next(k):
+        return {"ep": ((z + k) % depth) * 2 + y}
+
+    def fetch(s):
+        k, dy = (s // 2 + 1) % depth, 1 - s % 2
+        block = ((z + k) % depth) * 2 + (y + dy) % 2
+        span = 4 * rows
+        return pltpu.make_async_copy(
+            tokens_ref.at[pl.ds(pl.multiple_of(block * span, span), span)],
+            tokens.at[s % 2],
+            token_sem.at[s % 2],
+        )
+
+    def remote(source, target, send, recv, device):
+        return pltpu.make_async_remote_copy(
+            src_ref=source, dst_ref=target, send_sem=send, recv_sem=recv,
+            device_id=device, device_id_type=mesh_id,
+        )
+
+    def core_copy(s):
+        return remote(outgoing.at[s], incoming.at[s], core_send.at[s], core_recv.at[s], sibling)
+
+    def x_copy(s):
+        return remote(own.at[s, 0, 1], from_x.at[s], x_send.at[s], x_recv.at[s], x_next)
+
+    def y_copy(i):
+        return remote(own.at[2 * i, 1], from_y.at[i], y_send.at[i], y_recv.at[i], y_next)
+
+    def a_copy(i):
+        return remote(to_y.at[i], came_y.at[i], a_send.at[i], a_recv.at[i], y_next)
+
+    def b_copy(i):
+        return remote(to_x.at[i], came_x.at[i], b_send.at[i], b_recv.at[i], x_next)
+
+    def z_copy(i):
+        return remote(to_z.at[i], from_z.at[i], z_send.at[i], z_recv.at[i], z_next(i + 1))
+
+    fetch(0).start()
+    barrier = pltpu.get_barrier_semaphore()
+    partners = [sibling, x_next, y_next] + [z_next(k) for k in range(1, depth)]
+    for partner in partners:
+        pl.semaphore_signal(barrier, inc=1, device_id=partner, device_id_type=mesh_id)
+    pl.semaphore_wait(barrier, len(partners))
+
+    lane = lax.broadcasted_iota(jnp.int32, (rows, LANES), 1)
+    lane_value = lane.astype(jnp.float32)
+    slot_lane = lax.broadcasted_iota(jnp.int32, (capacity, LANES), 1)
+
+    def chosen_slots(table, expert):
+        column = jnp.sum(jnp.where(lane == expert, table, 0.0), axis=1, keepdims=True)
+        return jnp.where(column == lane_value, 1.0, 0.0)
+
+    def compute(s):
+        weights = []
+        for dx in (0, 1):
+            for q in (0, 1):
+                c = core if q == 0 else 1 - core
+                block = ((x + dx) % 2) * 2 + c
+                start = pl.multiple_of(block * rows, rows)
+                arrived = tokens[s % 2, pl.ds(start, rows), :]
+                table = arrived[:, features:].astype(jnp.float32)
+                picked = chosen_slots(table, ep)
+                if q == 0:
+                    place[s, dx] = picked.astype(jnp.bfloat16)
+                    place_next[s, dx] = chosen_slots(table, next_ep).astype(jnp.bfloat16)
+                select = picked.T[:capacity].astype(jnp.bfloat16)
+                taken = jnp.dot(select, arrived, preferred_element_type=jnp.float32)
+                first = (dx * 2 + q) * capacity
+                slots[first : first + capacity, :] = taken[:, :features].astype(jnp.bfloat16)
+                mine = (slot_lane == experts + ep) | (slot_lane == 2 * experts + ep)
+                weights.append(
+                    jnp.sum(jnp.where(mine, taken[:, features:], 0.0), axis=1, keepdims=True)
+                )
+        value = slots[...]
+        gate_h = jnp.dot(value, gate_ref[...], preferred_element_type=jnp.float32)
+        up_h = jnp.dot(value, up_ref[...], preferred_element_type=jnp.float32)
+        clipped = jnp.minimum(gate_h, clamp_top)
+        act = (
+            clipped
+            * jax.nn.sigmoid(sigmoid_sharp * clipped)
+            * (jnp.clip(up_h, -clamp_top, clamp_top) + 1.0)
+        ).astype(jnp.bfloat16)
+        for side in (0, 1):
+            columns = slice(side * half, (side + 1) * half)
+            part = jnp.dot(act, down_ref[:, columns], preferred_element_type=jnp.float32)
+            for dx in (0, 1):
+                for q in (0, 1):
+                    first = (dx * 2 + q) * capacity
+                    scaled = (part[first : first + capacity] * weights[dx * 2 + q]).astype(
+                        jnp.bfloat16
+                    )
+                    if q == 0:
+                        own[s, side, dx] = scaled
+                    else:
+                        outgoing[s, side, dx] = scaled
+
+    def spread_out(where, value):
+        return jnp.dot(where[:, :capacity], value, preferred_element_type=jnp.float32)
+
+    def step(s, carry):
+        @pl.when(s < steps)
+        def _():
+            @pl.when(s + 1 < steps)
+            def _():
+                fetch(s + 1).start()
+
+            fetch(s).wait()
+            compute(s)
+
+        @pl.when((s >= 1) & (s <= steps))
+        def _():
+            t = s - 1
+            core_copy(t).wait_recv()
+            for side in (0, 1):
+                for dx in (0, 1):
+                    own[t, side, dx] = (
+                        own[t, side, dx].astype(jnp.float32)
+                        + incoming[t, side, dx].astype(jnp.float32)
+                    ).astype(jnp.bfloat16)
+
+        @pl.when(s < steps)
+        def _():
+            core_copy(s).start()
+
+        i = (s - 4) // 2
+
+        @pl.when((s >= 4) & (s % 2 == 0) & (i < depth))
+        def _():
+            far, near = 2 * i, 2 * i + 1
+            x_copy(far).wait_recv()
+            where = place[far, 0]
+            to_y[i] = (spread_out(where, own[far, 0, 0]) + spread_out(where, from_x[far])).astype(
+                jnp.bfloat16
+            )
+            y_copy(i).wait_recv()
+            to_x[i] = (
+                spread_out(place[near, 1], own[near, 1, 1])
+                + spread_out(place_next[near, 1], from_y[i, 1])
+            ).astype(jnp.bfloat16)
+            x_copy(near).wait_recv()
+            where = place[near, 0]
+            keep_a[i] = spread_out(where, own[near, 0, 0]) + spread_out(where, from_x[near])
+            keep_b[i] = spread_out(where, own[near, 1, 0]) + spread_out(
+                place_next[near, 0], from_y[i, 0]
+            )
+            a_copy(i).start()
+            b_copy(i).start()
+
+        @pl.when((s >= 1) & (s <= steps))
+        def _():
+            t = s - 1
+            x_copy(t).start()
+
+            @pl.when(t % 2 == 0)
+            def _():
+                y_copy(t // 2).start()
+
+        j = (s - 6) // 2
+
+        @pl.when((s >= 6) & (s % 2 == 0) & (j < depth))
+        def _():
+            a_copy(j).wait_recv()
+            b_copy(j).wait_recv()
+            sum_a = keep_a[j] + came_y[j].astype(jnp.float32)
+            sum_b = keep_b[j] + came_x[j].astype(jnp.float32)
+
+            @pl.when(j < depth - 1)
+            def _():
+                to_z[j, :, :half] = sum_a.astype(jnp.bfloat16)
+                to_z[j, :, half:] = sum_b.astype(jnp.bfloat16)
+                z_copy(j).start()
+
+            @pl.when(j == depth - 1)
+            def _():
+                keep_a[j] = sum_a
+                keep_b[j] = sum_b
+
+        return carry
+
+    lax.fori_loop(0, 2 * depth + 5, step, 0)
+    for i in range(depth - 1):
+        z_copy(i).wait_recv()
+    for side, keep in ((0, keep_a), (1, keep_b)):
+        columns = slice(side * half, (side + 1) * half)
+        total = keep[depth - 1]
+        for i in range(depth - 1):
+            total = total + from_z[i, :, columns].astype(jnp.float32)
+        out_ref[:, columns] = total.astype(jnp.bfloat16)
+    for s in range(steps):
+        core_copy(s).wait_send()
+        x_copy(s).wait_send()
+    for i in range(depth):
+        y_copy(i).wait_send()
+        a_copy(i).wait_send()
+        b_copy(i).wait_send()
+    for i in range(depth - 1):
+        z_copy(i).wait_send()
+
+
+def dense_experts_fit(tok_rows, top_count, capacity):
+    experts = lax.axis_size("ep")
+    fits = experts % 2 == 0 and experts >= 4 and 3 * experts <= LANES and lax.axis_size("tp") == 4
+    return fits and 2 * top_count >= experts and tok_rows == LANES and capacity % 16 == 0
+
+
+def gathered_tokens(
+    specialist_sample_slice, specialist_scaling_vector, chosen_specialists, dispatcher_affinity_matrix
+):
+    rows, features = specialist_sample_slice.shape
+    marked = pl.pallas_call(
+        functools.partial(routing_kernel, lax.axis_size("ep")),
+        out_shape=jax.ShapeDtypeStruct((rows, features + LANES), jnp.bfloat16),
+        name="routing",
+    )(
+        specialist_sample_slice, specialist_scaling_vector[None], chosen_specialists,
+        dispatcher_affinity_matrix,
+    )
+    return lax.all_gather(marked, ("ep", "tp"), axis=0, tiled=True)
+
+
+def experts_dense(
+    tokens, rows, capacity, gating_projection, expand_projection, shrink_projection
+):
+    experts = lax.axis_size("ep")
+    features = gating_projection.shape[1]
+    half, depth, steps = features // 2, experts // 2, experts
+    hidden = gating_projection.shape[2]
+    narrow = jnp.bfloat16
+    dma = pltpu.SemaphoreType.DMA
+    work = 2 * experts * 4 * capacity * features * hidden * 3
+    return pl.pallas_call(
+        functools.partial(experts_kernel, experts, capacity),
+        in_specs=[pl.BlockSpec(memory_space=pl.ANY)]
+        + [pl.BlockSpec(memory_space=pltpu.VMEM)] * 3,
+        out_specs=pl.BlockSpec(memory_space=pltpu.VMEM),
+        out_shape=jax.ShapeDtypeStruct((rows, features), narrow),
+        scratch_shapes=[
+            pltpu.VMEM((2, 4 * rows, features + LANES), narrow),
+            pltpu.VMEM((4 * capacity, features), narrow),
+            pltpu.VMEM((steps, 2, 2, capacity, half), narrow),
+            pltpu.VMEM((steps, 2, 2, capacity, half), narrow),
+            pltpu.VMEM((steps, 2, 2, capacity, half), narrow),
+            pltpu.VMEM((steps, 2, rows, LANES), narrow),
+            pltpu.VMEM((steps, 2, rows, LANES), narrow),
+            pltpu.VMEM((steps, capacity, half), narrow),
+            pltpu.VMEM((depth, 2, capacity, half), narrow),
+            pltpu.VMEM((depth, rows, half), narrow),
+            pltpu.VMEM((depth, rows, half), narrow),
+            pltpu.VMEM((depth, rows, half), narrow),
+            pltpu.VMEM((depth, rows, half), narrow),
+            pltpu.VMEM((depth, rows, half), jnp.float32),
+            pltpu.VMEM((depth, rows, half), jnp.float32),
+            pltpu.VMEM((depth - 1, rows, features), narrow),
+            pltpu.VMEM((depth - 1, rows, features), narrow),
+            dma((2,)), dma((steps,)), dma((steps,)), dma((steps,)), dma((steps,)),
+            dma((depth,)), dma((depth,)), dma((depth,)), dma((depth,)), dma((depth,)),
+            dma((depth,)), dma((depth - 1,)), dma((depth - 1,)),
+        ],
+        compiler_params=pltpu.CompilerParams(
+            collective_id=0, has_side_effects=True, vmem_limit_bytes=60 * 1024 * 1024
+        ),
+        cost_estimate=pl.CostEstimate(
+            flops=8 * work, bytes_accessed=4 * tokens.size, transcendentals=0
+        ),
+        name="experts",
+    )(tokens, gating_projection[0], expand_projection[0], shrink_projection[0])
+
+
 def body(
     sequence_entry_features,
     sequence_exit_gating,
@@ -366,6 +688,16 @@
     expand_projection,
     shrink_projection,
 ):
+    tok_rows, top_count = chosen_specialists.shape
+    capacity = tok_rows * top_count * 5 // (4 * lax.axis_size("ep"))
+    dense = dense_experts_fit(tok_rows, top_count, capacity)
+    if dense:
+        tokens = gathered_tokens(
+            specialist_sample_slice,
+            specialist_scaling_vector,
+            chosen_specialists,
+            dispatcher_affinity_matrix,
+        )
     mixed = mixer_half(
         sequence_entry_features,
         sequence_exit_gating,
@@ -382,6 +714,11 @@
         cluster_scaling_vector,
         sequence_exit_projection,
     )
+    if dense:
+        moe_out = experts_dense(
+            tokens, tok_rows, capacity, gating_projection, expand_projection, shrink_projection
+        )
+        return (mixed, moe_out)
     moe_out = experts_half(
         specialist_sample_slice,
         specialist_scaling_vector,

time: 388 us -> 295 us (0.76)
  Pallas kernels: 41.9 us -> 177 us
  waiting for transfers between devices: 146 us -> 37.4 us
  blocking collectives: 66.9 us -> 0 us
  matrix products: 43.2 us -> 11.6 us
  local copies, waits for them, and re-layouts: 27 us -> 12.8 us
  other arithmetic: 11.6 us -> 5.54 us
    pallas_call x0 -> x2, Pallas kernels: none -> 135 us  [the longest x1 133 us: experts_dense(): pl.pallas_call(functools.partial(experts_kernel, experts, capacity), in_s...]
    all_gather x1, waiting for transfers between devices: 69.3 us -> 0.02 us  [gathered_tokens(): return lax.all_gather(marked, ('ep', 'tp'), axis=0, tiled=True)]
    all_to_all x1 -> x0, blocking collectives: 66.9 us -> none  [experts_half(): lax.all_to_all(outgoing, 'ep', split_axis=0, concat_axis=0, tiled=True)]
    all_to_all x1 -> x0, waiting for transfers between devices: 58.7 us -> none  [experts_half(): lax.all_to_all(summed.reshape(experts, capacity, feature_count), 'ep', sp...]
    dot_general x3 -> x0, matrix products: 31.8 us -> none  [the longest x1 18.5 us: experts_half(): jnp.dot(hidden_act, shrink_projection[0], preferred_element_type=jnp.floa...]
    ppermute x5, waiting for transfers between devices: 17.6 us -> 37.3 us  [passed_along(): return lax.ppermute(block, axis, route)]
    all_to_all x1 -> x0, starting transfers between devices: 16 us -> none  [experts_half(): lax.all_to_all(summed.reshape(experts, capacity, feature_count), 'ep', sp...]
    ppermute x5, starting transfers between devices: 20.3 us -> 33.8 us  [passed_along(): return lax.ppermute(block, axis, route)]
  transfers between devices with their start and end apart: 9 -> 7, of which waited for: 6 -> 4; matrix products, arithmetic and copies ran while one was open for 10% -> 9% of each run, Pallas kernels for 11% -> 59%
where the time goes in v1:
time: 295 us; the launch traced here: 294 us
  Pallas kernels  177 us (60%)
  waiting for transfers between devices  37.4 us (13%)
  starting transfers between devices  33.8 us (11%)
  between operations  15.7 us (5%)
  local copies, waits for them, and re-layouts  12.8 us (4%)
  matrix products  11.6 us (4%)
  other arithmetic  5.54 us (2%)
    pallas_call x1, Pallas kernels, experts_dense(): pl.pallas_call(functools.partial(experts_kernel, experts, capacity), in_s...  133 us
    ppermute x5, waiting for transfers between devices, passed_along(): return lax.ppermute(block, axis, route)  37.3 us
    ppermute x5, starting transfers between devices, passed_along(): return lax.ppermute(block, axis, route)  33.8 us
    pallas_call x1, Pallas kernels, mixer_half(): pl.pallas_call(functools.partial(output_kernel, per_group, local_groups),...  25.6 us
    pallas_call x1, Pallas kernels, mixer_half(): pl.pallas_call(functools.partial(state_kernel, per_group, local_groups),...  16.1 us
    dot_general x1, matrix products, mixer_half(): jnp.dot(normed, sequence_exit_projection, preferred_element_type=jnp.floa...  11.4 us
  transfers between devices with their start and end apart: 7, of which 4 were waited for; matrix products, arithmetic and copies ran while one was open for 9% of the time, Pallas kernels for 59%

profile of v1, /device:TPU:0, one launch (start us, length us, event | category | flops | bytes accessed | tf_op | source)
XLA Modules:
  0.0 294.0 jit_solution(295465298878801584)
XLA Ops:
  8.0 1.4 copy.33.chosen_ref
  9.5 1.4 copy.34.score_ref
  10.9 2.5 routing.1
  13.5 0.7 slice.38
  14.1 0.7 slice.37
  14.8 0.7 slice.36
  15.6 4.9 %collective-permute-start = (bf16[8,1536]{1,0:T(8,128)(2,1)S(1)}, bf16[8,1536]{1,0:T(8,128)(2,1)S(1)}, u32[]{:S(2)}, u32[]{:S(2)}) collective-permute-start(bf16[8,1536]{1,0:T(8,128)(2,1)S(1)} %pad_maximum_fusion.3), channel_id=1, source_target_pairs={{0,4},{4,8},{8,12},{12,16},{16,20},{20,24},{24,28},{1,5},{5,9},{9,... | collective-permute-start | bytes 73736 | tf_op jit(solution)/shard_map/ppermute | solution.py:24
  20.5 0.7 exp.19
  21.1 1.1 log_bitcast_fusion
  22.7 0.7 fusion.6
  23.7 0.7 broadcast_in_dim.57.end_ref
  24.4 1.2 copy.36
  25.5 0.6 slice.48.xr_ref
  26.1 0.6 fusion.13
  26.7 16.1 %own_state.1 = f32[128,1024]{1,0:T(8,128)} custom-call(bf16[1536,1024]{1,0:T(8,128)(2,1)} %x_ref.4, bf16[8,1024]{1,0:T(8,128)(2,1)} %slice.48.xr_ref, bf16[4,1024]{1,0:T(4,128)(2,1)} %xt_ref.3, bf16[1536,256]{1,0:T(8,128)(2,1)} %b_ref.3, bf16[8,256]{1,0:T(8,128)(2,1)} %get-tuple-element.10.br_ref, bf16[4,256]{1,0:T(4,128)(2,1)} %bt_ref.3, ...), custom_call_target="tpu_custom_call" | custom-call | flops 1610612736 | bytes 12582912 | tf_op jit(solution)/shard_map/own_state/pallas_call | solution.py:222
  42.9 1.1 convert.21
  44.1 3.4 %collective-permute-start.1 = (bf16[136,1024]{1,0:T(8,128)(2,1)S(1)}, bf16[136,1024]{1,0:T(8,128)(2,1)S(1)}, u32[]{:S(2)}, u32[]{:S(2)}) collective-permute-start(bf16[136,1024]{1,0:T(8,128)(2,1)S(1)} %pad_maximum_fusion), channel_id=1, source_target_pairs={{0,4},{4,8},{8,12},{12,16},{16,20},{20,24},{24,28},{1,5},{5,9},{9,... | collective-permute-start | bytes 835592 | tf_op jit(solution)/shard_map/ppermute | solution.py:24
  47.6 12.3 %collective-permute-done.1 = bf16[136,1024]{1,0:T(8,128)(2,1)S(1)} collective-permute-done((bf16[136,1024]{1,0:T(8,128)(2,1)S(1)}, bf16[136,1024]{1,0:T(8,128)(2,1)S(1)}, u32[]{:S(2)}, u32[]{:S(2)}) %collective-permute-start.1) | collective-permute-done | bytes 278560 | tf_op jit(solution)/shard_map/ppermute | solution.py:24
  59.9 1.1 fusion
  61.1 5.5 %collective-permute-start.2 = (bf16[136,1024]{1,0:T(8,128)(2,1)S(1)}, bf16[136,1024]{1,0:T(8,128)(2,1)S(1)}, u32[]{:S(2)}, u32[]{:S(2)}) collective-permute-start(bf16[136,1024]{1,0:T(8,128)(2,1)S(1)} %pad_maximum_fusion.1), channel_id=1, source_target_pairs={{0,8},{4,12},{8,16},{12,20},{16,24},{20,28},{1,9},{5,13},{9,17},{1... | collective-permute-start | bytes 835592 | tf_op jit(solution)/shard_map/ppermute | solution.py:24
  66.5 11.6 %collective-permute-done.2 = bf16[136,1024]{1,0:T(8,128)(2,1)S(1)} collective-permute-done((bf16[136,1024]{1,0:T(8,128)(2,1)S(1)}, bf16[136,1024]{1,0:T(8,128)(2,1)S(1)}, u32[]{:S(2)}, u32[]{:S(2)}) %collective-permute-start.2) | collective-permute-done | bytes 278560 | tf_op jit(solution)/shard_map/ppermute | solution.py:24
  78.4 5.6 %collective-permute-start.3 = (bf16[136,1024]{1,0:T(8,128)(2,1)S(1)}, bf16[136,1024]{1,0:T(8,128)(2,1)S(1)}, u32[]{:S(2)}, u32[]{:S(2)}) collective-permute-start(bf16[136,1024]{1,0:T(8,128)(2,1)S(1)} %pad_maximum_fusion.2), channel_id=1, source_target_pairs={{0,16},{4,20},{8,24},{12,28},{1,17},{5,21},{9,25},{13,29},{2,18},{... | collective-permute-start | bytes 835592 | tf_op jit(solution)/shard_map/ppermute | solution.py:24
  84.0 4.4 %collective-permute-done.3 = bf16[136,1024]{1,0:T(8,128)(2,1)S(1)} collective-permute-done((bf16[136,1024]{1,0:T(8,128)(2,1)S(1)}, bf16[136,1024]{1,0:T(8,128)(2,1)S(1)}, u32[]{:S(2)}, u32[]{:S(2)}) %collective-permute-start.3) | collective-permute-done | bytes 278560 | tf_op jit(solution)/shard_map/ppermute | solution.py:24
  88.6 14.4 %collective-permute-start.4 = (bf16[128,1024]{1,0:T(8,128)(2,1)S(1)}, bf16[128,1024]{1,0:T(8,128)(2,1)S(1)}, u32[]{:S(2)}, u32[]{:S(2)}) collective-permute-start(bf16[128,1024]{1,0:T(8,128)(2,1)S(1)} %add_convert_fusion), channel_id=1, source_target_pairs={{0,4},{4,8},{8,12},{12,16},{16,20},{20,24},{24,28},{1,5},{5,9},{9,... | collective-permute-start | bytes 786440 | tf_op jit(solution)/shard_map/ppermute | solution.py:24
  103.0 1.2 copy.35
  104.3 0.7 broadcast_in_dim_reshape.3.skip_ref
  104.9 9.0 %collective-permute-done.4 = bf16[128,1024]{1,0:T(8,128)(2,1)S(1)} collective-permute-done((bf16[128,1024]{1,0:T(8,128)(2,1)S(1)}, bf16[128,1024]{1,0:T(8,128)(2,1)S(1)}, u32[]{:S(2)}, u32[]{:S(2)}) %collective-permute-start.4) | collective-permute-done | bytes 262176 | tf_op jit(solution)/shard_map/ppermute | solution.py:24
  113.9 0.8 convert_element_type.37.enter_ref
  114.7 25.6 %mixer_output.1 = bf16[1536,1024]{1,0:T(8,128)(2,1)} custom-call(bf16[1536,1024]{1,0:T(8,128)(2,1)} %x_ref.4, bf16[8,1024]{1,0:T(8,128)(2,1)} %slice.48.xr_ref, bf16[4,1024]{1,0:T(4,128)(2,1)} %xt_ref.3, bf16[1536,256]{1,0:T(8,128)(2,1)} %b_ref.3, bf16[8,256]{1,0:T(8,128)(2,1)} %get-tuple-element.10.br_ref, bf16[4,256]{1,0:T(4,128)(2,1)} %bt_ref.3, ...), custom_call_target="tpu_custom_call" | custom-call | flops 4831838208 | bytes 37748736 | tf_op jit(solution)/shard_map/mixer_output/pallas_call | solution.py:236
  140.4 11.4 %convolution_convert_fusion = bf16[1536,2048]{1,0:T(8,128)(2,1)} fusion(bf16[1536,1024]{1,0:T(8,128)(2,1)} %mixer_output.1, bf16[1024,2048]{1,0:T(8,128)(2,1)} %param.34), kind=kOutput, calls=%fused_computation | convolution fusion | flops 6445596672 | bytes 13631488 | tf_op jit(solution)/shard_map/dot_general | solution.py:265
  151.8 132.8 %experts.1 = bf16[128,2048]{1,0:T(8,128)(2,1)} custom-call(bf16[4096,2176]{1,0:T(8,128)(2,1)} %all-gather.2.cloned.1.call-done.tokens_ref, bf16[2048,512]{1,0:T(8,128)(2,1)} %bitcast.40, bf16[2048,512]{1,0:T(8,128)(2,1)} %bitcast.41, bf16[512,2048]{1,0:T(8,128)(2,1)} %bitcast.42), custom_call_target="tpu_custom_call" | custom-call | flops 128849018880 | bytes 35651584 | tf_op jit(solution)/shard_map/experts/pallas_call | solution.py:630
  284.7 1.9 copy.51
  (33 shorter events, 1.5 us)
Async XLA Ops:
  8.0 143.8 %all-gather.2.cloned.1.call-start = ((), (), s32[]{:S(2)}) async-start(), calls=%async_computation.2 | async-start | bytes 18382848 | tf_op jit(solution)/shard_map/all_gather | solution.py:617
  13.4 271.3 %reduce-scatter.2.cloned.1.call-start = ((), (), s32[]{:S(2)}) async-start(), calls=%async_computation.1 | async-start | bytes 7864320 | tf_op jit(solution)/shard_map/reduce_scatter | solution.py:264
  15.6 10.0 %collective-permute-start = (bf16[8,1536]{1,0:T(8,128)(2,1)S(1)}, bf16[8,1536]{1,0:T(8,128)(2,1)S(1)}, u32[]{:S(2)}, u32[]{:S(2)}) collective-permute-start(bf16[8,1536]{1,0:T(8,128)(2,1)S(1)} %pad_maximum_fusion.3), channel_id=1, source_target_pairs={{0,4},{4,8},{8,12},{12,16},{16,20},{20,24},{24,28},{1,5},{5,9},{9,... | collective-permute-start | bytes 73736 | tf_op jit(solution)/shard_map/ppermute | solution.py:24
  42.8 35.3 %copy-start = (f32[128,1024]{1,0:T(8,128)S(1)}, f32[128,1024]{1,0:T(8,128)}, u32[]{:S(2)}) copy-start(f32[128,1024]{1,0:T(8,128)} %own_state.1) | copy-start | bytes 1572868
  44.0 60.2 %copy-start.1 = (f32[16]{0:T(128)S(1)}, f32[16]{0:T(128)}, u32[]{:S(2)}) copy-start(f32[16]{0:T(128)} %param.31) | copy-start | bytes 196
  44.1 15.8 %collective-permute-start.1 = (bf16[136,1024]{1,0:T(8,128)(2,1)S(1)}, bf16[136,1024]{1,0:T(8,128)(2,1)S(1)}, u32[]{:S(2)}, u32[]{:S(2)}) collective-permute-start(bf16[136,1024]{1,0:T(8,128)(2,1)S(1)} %pad_maximum_fusion), channel_id=1, source_target_pairs={{0,4},{4,8},{8,12},{12,16},{16,20},{20,24},{24,28},{1,5},{5,9},{9,... | collective-permute-start | bytes 835592 | tf_op jit(solution)/shard_map/ppermute | solution.py:24
  61.1 17.1 %collective-permute-start.2 = (bf16[136,1024]{1,0:T(8,128)(2,1)S(1)}, bf16[136,1024]{1,0:T(8,128)(2,1)S(1)}, u32[]{:S(2)}, u32[]{:S(2)}) collective-permute-start(bf16[136,1024]{1,0:T(8,128)(2,1)S(1)} %pad_maximum_fusion.1), channel_id=1, source_target_pairs={{0,8},{4,12},{8,16},{12,20},{16,24},{20,28},{1,9},{5,13},{9,17},{1... | collective-permute-start | bytes 835592 | tf_op jit(solution)/shard_map/ppermute | solution.py:24
  78.4 10.0 %collective-permute-start.3 = (bf16[136,1024]{1,0:T(8,128)(2,1)S(1)}, bf16[136,1024]{1,0:T(8,128)(2,1)S(1)}, u32[]{:S(2)}, u32[]{:S(2)}) collective-permute-start(bf16[136,1024]{1,0:T(8,128)(2,1)S(1)} %pad_maximum_fusion.2), channel_id=1, source_target_pairs={{0,16},{4,20},{8,24},{12,28},{1,17},{5,21},{9,25},{13,29},{2,18},{... | collective-permute-start | bytes 835592 | tf_op jit(solution)/shard_map/ppermute | solution.py:24
  88.6 25.3 %collective-permute-start.4 = (bf16[128,1024]{1,0:T(8,128)(2,1)S(1)}, bf16[128,1024]{1,0:T(8,128)(2,1)S(1)}, u32[]{:S(2)}, u32[]{:S(2)}) collective-permute-start(bf16[128,1024]{1,0:T(8,128)(2,1)S(1)} %add_convert_fusion), channel_id=1, source_target_pairs={{0,4},{4,8},{8,12},{12,16},{16,20},{20,24},{24,28},{1,5},{5,9},{9,... | collective-permute-start | bytes 786440 | tf_op jit(solution)/shard_map/ppermute | solution.py:24
Sparse Core Ops, SparseCore 0:
  13.5 132.1 all-gather.1
Sparse Core Ops, SparseCore 1:
  151.8 117.7 reduce-scatter.1

commit v2 on v1

--- a/solution.py
+++ b/solution.py
@@ -11,6 +11,7 @@
 SPAN = 128
 RIM = 8
 LANES = 128
+MIX_ROWS = 32
 
 norm_eps = 1e-05
 clamp_top = 7.0
@@ -261,13 +262,8 @@
         *x_args, *b_args, *c_args, sequence_exit_gating, key_log, cumulative, row_log, end_factor,
         entering, jnp.repeat(skip_connection_factor, HEAD)[None], cluster_scaling_vector[None],
     )
-    return lax.psum_scatter(
-        jnp.dot(normed, sequence_exit_projection, preferred_element_type=jnp.float32).astype(
-            jnp.bfloat16
-        ),
-        "tp",
-        scatter_dimension=0,
-        tiled=True,
+    return jnp.dot(normed, sequence_exit_projection, preferred_element_type=jnp.float32).astype(
+        jnp.bfloat16
     )
 
 
@@ -378,9 +374,10 @@
 
 
 def experts_kernel(
-    experts, capacity, tokens_ref, gate_ref, up_ref, down_ref, out_ref,
+    experts, capacity, tokens_ref, mix_ref, gate_ref, up_ref, down_ref, out_ref, mixed_ref,
     tokens, slots, own, outgoing, incoming, place, place_next, from_x, from_y,
     to_y, came_y, to_x, came_x, keep_a, keep_b, to_z, from_z,
+    mix_own, mix_core, mix_out, mix_in, mix_sem, mc_send, mc_recv, mx_send, mx_recv,
     token_sem, core_send, core_recv, x_send, x_recv, y_send, y_recv,
     a_send, a_recv, b_send, b_recv, z_send, z_recv,
 ):
@@ -434,12 +431,64 @@
     def z_copy(i):
         return remote(to_z.at[i], from_z.at[i], z_send.at[i], z_recv.at[i], z_next(i + 1))
 
+    chunks, piece = mixed_ref.shape[0] // MIX_ROWS, MIX_ROWS
+    share = mixed_ref.shape[0]
+
+    def mix_rows(dx, c):
+        block = ((x + dx) % 2) * 2 + c
+        return mix_ref.at[pl.ds(pl.multiple_of(block * share, share), share)]
+
+    def mix_fetch(dx):
+        return pltpu.make_async_copy(mix_rows(dx, core), mix_own.at[dx], mix_sem.at[dx])
+
+    def mix_core_copy(dx):
+        return remote(
+            mix_rows(dx, 1 - core), mix_core.at[dx], mc_send.at[dx], mc_recv.at[dx], sibling
+        )
+
+    def mix_x_copy(j):
+        rows_j = pl.ds(pl.multiple_of(j * piece, piece), piece)
+        return remote(
+            mix_out.at[rows_j], mix_in.at[rows_j], mx_send.at[j], mx_recv.at[j], x_next
+        )
+
+    def mix_piece(j, carry):
+        rows_j = pl.ds(pl.multiple_of(j * piece, piece), piece)
+        mix_out[rows_j, :] = (
+            mix_own[1, rows_j, :].astype(jnp.float32) + mix_core[1, rows_j, :].astype(jnp.float32)
+        ).astype(jnp.bfloat16)
+        mix_own[0, rows_j, :] = (
+            mix_own[0, rows_j, :].astype(jnp.float32) + mix_core[0, rows_j, :].astype(jnp.float32)
+        ).astype(jnp.bfloat16)
+        return carry
+
+    def mix_send(j, carry):
+        mix_x_copy(j).start()
+        return carry
+
+    def mix_finish(j, carry):
+        rows_j = pl.ds(pl.multiple_of(j * piece, piece), piece)
+        mix_x_copy(j).wait_recv()
+        mixed_ref[rows_j, :] = (
+            mix_own[0, rows_j, :].astype(jnp.float32) + mix_in[rows_j, :].astype(jnp.float32)
+        ).astype(jnp.bfloat16)
+        return carry
+
+    def mix_sent(j, carry):
+        mix_x_copy(j).wait_send()
+        return carry
+
     fetch(0).start()
+    for dx in (1, 0):
+        mix_fetch(dx).start()
     barrier = pltpu.get_barrier_semaphore()
     partners = [sibling, x_next, y_next] + [z_next(k) for k in range(1, depth)]
     for partner in partners:
         pl.semaphore_signal(barrier, inc=1, device_id=partner, device_id_type=mesh_id)
     pl.semaphore_wait(barrier, len(partners))
+
+    for dx in (1, 0):
+        mix_core_copy(dx).start()
 
     lane = lax.broadcasted_iota(jnp.int32, (rows, LANES), 1)
     lane_value = lane.astype(jnp.float32)
@@ -496,6 +545,8 @@
     def spread_out(where, value):
         return jnp.dot(where[:, :capacity], value, preferred_element_type=jnp.float32)
 
+    last_x = 2 * depth + 2
+
     def step(s, carry):
         @pl.when(s < steps)
         def _():
@@ -520,6 +571,13 @@
         @pl.when(s < steps)
         def _():
             core_copy(s).start()
+
+        @pl.when(s == 0)
+        def _():
+            for dx in (1, 0):
+                mix_fetch(dx).wait()
+                mix_core_copy(dx).wait_recv()
+            lax.fori_loop(0, chunks, mix_piece, 0)
 
         i = (s - 4) // 2
 
@@ -554,6 +612,16 @@
             def _():
                 y_copy(t // 2).start()
 
+        early, late = chunks // 4, chunks // 2
+        begin = jnp.where(s == 0, 0, jnp.where(s < last_x, early + s - 3, late))
+        end = jnp.where(s == 0, early, jnp.where(s < last_x, early + s - 2, chunks))
+        lax.fori_loop(
+            jnp.where((s == 0) | (s == last_x), begin, jnp.clip(begin, early, late)),
+            jnp.where((s == 0) | (s == last_x), end,
+                      jnp.where(s > last_x, 0, jnp.clip(end, early, late))),
+            mix_send, 0,
+        )
+
         j = (s - 6) // 2
 
         @pl.when((s >= 6) & (s % 2 == 0) & (j < depth))
@@ -585,6 +653,10 @@
         for i in range(depth - 1):
             total = total + from_z[i, :, columns].astype(jnp.float32)
         out_ref[:, columns] = total.astype(jnp.bfloat16)
+    lax.fori_loop(0, chunks, mix_finish, 0)
+    lax.fori_loop(0, chunks, mix_sent, 0)
+    for dx in (0, 1):
+        mix_core_copy(dx).wait_send()
     for s in range(steps):
         core_copy(s).wait_send()
         x_copy(s).wait_send()
@@ -596,10 +668,10 @@
         z_copy(i).wait_send()
 
 
-def dense_experts_fit(tok_rows, top_count, capacity):
+def dense_experts_fit(tok_rows, top_count, capacity, mix_rows):
     experts = lax.axis_size("ep")
     fits = experts % 2 == 0 and experts >= 4 and 3 * experts <= LANES and lax.axis_size("tp") == 4
-    return fits and 2 * top_count >= experts and tok_rows == LANES and capacity % 16 == 0
+    return fits and 2 * top_count >= experts and mix_rows % (4 * MIX_ROWS) == 0 and tok_rows == LANES and capacity % 16 == 0
 
 
 def gathered_tokens(
@@ -618,7 +690,7 @@
 
 
 def experts_dense(
-    tokens, rows, capacity, gating_projection, expand_projection, shrink_projection
+    tokens, mix_part, rows, capacity, gating_projection, expand_projection, shrink_projection
 ):
     experts = lax.axis_size("ep")
     features = gating_projection.shape[1]
@@ -626,13 +698,18 @@
     hidden = gating_projection.shape[2]
     narrow = jnp.bfloat16
     dma = pltpu.SemaphoreType.DMA
+    share = mix_part.shape[0] // 4
+    pieces = share // MIX_ROWS
     work = 2 * experts * 4 * capacity * features * hidden * 3
     return pl.pallas_call(
         functools.partial(experts_kernel, experts, capacity),
-        in_specs=[pl.BlockSpec(memory_space=pl.ANY)]
+        in_specs=[pl.BlockSpec(memory_space=pl.ANY)] * 2
         + [pl.BlockSpec(memory_space=pltpu.VMEM)] * 3,
-        out_specs=pl.BlockSpec(memory_space=pltpu.VMEM),
-        out_shape=jax.ShapeDtypeStruct((rows, features), narrow),
+        out_specs=[pl.BlockSpec(memory_space=pltpu.VMEM)] * 2,
+        out_shape=[
+            jax.ShapeDtypeStruct((rows, features), narrow),
+            jax.ShapeDtypeStruct((share, features), narrow),
+        ],
         scratch_shapes=[
             pltpu.VMEM((2, 4 * rows, features + LANES), narrow),
             pltpu.VMEM((4 * capacity, features), narrow),
@@ -651,18 +728,23 @@
             pltpu.VMEM((depth, rows, half), jnp.float32),
             pltpu.VMEM((depth - 1, rows, features), narrow),
             pltpu.VMEM((depth - 1, rows, features), narrow),
+            pltpu.VMEM((2, share, features), narrow),
+            pltpu.VMEM((2, share, features), narrow),
+            pltpu.VMEM((share, features), narrow),
+            pltpu.VMEM((share, features), narrow),
+            dma((2,)), dma((2,)), dma((2,)), dma((pieces,)), dma((pieces,)),
             dma((2,)), dma((steps,)), dma((steps,)), dma((steps,)), dma((steps,)),
             dma((depth,)), dma((depth,)), dma((depth,)), dma((depth,)), dma((depth,)),
             dma((depth,)), dma((depth - 1,)), dma((depth - 1,)),
         ],
         compiler_params=pltpu.CompilerParams(
-            collective_id=0, has_side_effects=True, vmem_limit_bytes=60 * 1024 * 1024
+            collective_id=0, has_side_effects=True, vmem_limit_bytes=63 * 1024 * 1024
         ),
         cost_estimate=pl.CostEstimate(
             flops=8 * work, bytes_accessed=4 * tokens.size, transcendentals=0
         ),
         name="experts",
-    )(tokens, gating_projection[0], expand_projection[0], shrink_projection[0])
+    )(tokens, mix_part, gating_projection[0], expand_projection[0], shrink_projection[0])
 
 
 def body(
@@ -690,7 +772,7 @@
 ):
     tok_rows, top_count = chosen_specialists.shape
     capacity = tok_rows * top_count * 5 // (4 * lax.axis_size("ep"))
-    dense = dense_experts_fit(tok_rows, top_count, capacity)
+    dense = dense_experts_fit(tok_rows, top_count, capacity, sequence_entry_features.shape[0])
     if dense:
         tokens = gathered_tokens(
             specialist_sample_slice,
@@ -698,7 +780,7 @@
             chosen_specialists,
             dispatcher_affinity_matrix,
         )
-    mixed = mixer_half(
+    mix_part = mixer_half(
         sequence_entry_features,
         sequence_exit_gating,
         memory_insert_clusters,
@@ -715,10 +797,11 @@
         sequence_exit_projection,
     )
     if dense:
-        moe_out = experts_dense(
-            tokens, tok_rows, capacity, gating_projection, expand_projection, shrink_projection
+        moe_out, mixed = experts_dense(
+            tokens, mix_part, tok_rows, capacity, gating_projection, expand_projection, shrink_projection
         )
         return (mixed, moe_out)
+    mixed = lax.psum_scatter(mix_part, "tp", scatter_dimension=0, tiled=True)
     moe_out = experts_half(
         specialist_sample_slice,
         specialist_scaling_vector,

time: 295 us -> 291 us (0.986)
  Pallas kernels: 177 us -> 173 us
    pallas_call x1, Pallas kernels: 133 us -> 128 us  [experts_dense(): pl.pallas_call(functools.partial(experts_kernel, experts, capacity), in_s...]
    unnamed x7 -> x10, local copies, waits for them, and re-layouts: 4.72 us -> 6.42 us
  transfers between devices with their start and end apart: 7 -> 6, of which waited for: 4 -> 4; matrix products, arithmetic and copies ran while one was open for 9% -> 9% of each run, Pallas kernels for 59% -> 14%
where the time goes in v2:
time: 291 us; the launch traced here: 290 us
  Pallas kernels  173 us (59%)
  waiting for transfers between devices  37.5 us (13%)
  starting transfers between devices  33.8 us (12%)
  local copies, waits for them, and re-layouts  14.5 us (5%)
  between operations  14.2 us (5%)
  matrix products  11.7 us (4%)
  other arithmetic  5.54 us (2%)
    pallas_call x1, Pallas kernels, experts_dense(): pl.pallas_call(functools.partial(experts_kernel, experts, capacity), in_s...  128 us
    ppermute x5, waiting for transfers between devices, passed_along(): return lax.ppermute(block, axis, route)  37.5 us
    ppermute x5, starting transfers between devices, passed_along(): return lax.ppermute(block, axis, route)  33.8 us
    pallas_call x1, Pallas kernels, mixer_half(): pl.pallas_call(functools.partial(output_kernel, per_group, local_groups),...  25.6 us
    pallas_call x1, Pallas kernels, mixer_half(): pl.pallas_call(functools.partial(state_kernel, per_group, local_groups),...  16.1 us
    dot_general x1, matrix products, mixer_half(): jnp.dot(normed, sequence_exit_projection, preferred_element_type=jnp.floa...  11.4 us
    unnamed x10, local copies, waits for them, and re-layouts  6.42 us
  transfers between devices with their start and end apart: 6, of which 4 were waited for; matrix products, arithmetic and copies ran while one was open for 9% of the time, Pallas kernels for 14%

profile of v2, /device:TPU:0, one launch (start us, length us, event | category | flops | bytes accessed | tf_op | source)
XLA Modules:
  0.0 290.0 jit_solution(8622618741087055203)
XLA Ops:
  7.2 1.4 copy.26.chosen_ref
  8.6 1.4 copy.27.score_ref
  10.0 2.5 routing.1
  12.6 0.7 slice.36
  13.3 0.7 slice.37
  14.0 0.7 slice.38
  14.7 4.9 %collective-permute-start = (bf16[8,1536]{1,0:T(8,128)(2,1)S(1)}, bf16[8,1536]{1,0:T(8,128)(2,1)S(1)}, u32[]{:S(2)}, u32[]{:S(2)}) collective-permute-start(bf16[8,1536]{1,0:T(8,128)(2,1)S(1)} %pad_maximum_fusion.3), channel_id=1, source_target_pairs={{0,4},{4,8},{8,12},{12,16},{16,20},{20,24},{24,28},{1,5},{5,9},{9,... | collective-permute-start | bytes 73736 | tf_op jit(solution)/shard_map/ppermute | solution.py:25
  19.6 0.7 exp.19
  20.2 1.1 log_bitcast_fusion
  21.8 0.7 fusion.6
  22.5 1.2 copy.36
  23.7 0.7 broadcast_in_dim.58.end_ref
  24.6 0.6 slice.48.xr_ref
  25.8 16.1 %own_state.1 = f32[128,1024]{1,0:T(8,128)} custom-call(bf16[1536,1024]{1,0:T(8,128)(2,1)} %x_ref.5, bf16[8,1024]{1,0:T(8,128)(2,1)} %slice.48.xr_ref, bf16[4,1024]{1,0:T(4,128)(2,1)} %xt_ref.3, bf16[1536,256]{1,0:T(8,128)(2,1)} %b_ref.3, bf16[8,256]{1,0:T(8,128)(2,1)} %get-tuple-element.14.br_ref, bf16[4,256]{1,0:T(4,128)(2,1)} %bt_ref.3, ...), custom_call_target="tpu_custom_call" | custom-call | flops 1610612736 | bytes 12582912 | tf_op jit(solution)/shard_map/own_state/pallas_call | solution.py:223
  41.9 1.1 convert.21
  43.1 3.4 %collective-permute-start.1 = (bf16[136,1024]{1,0:T(8,128)(2,1)S(1)}, bf16[136,1024]{1,0:T(8,128)(2,1)S(1)}, u32[]{:S(2)}, u32[]{:S(2)}) collective-permute-start(bf16[136,1024]{1,0:T(8,128)(2,1)S(1)} %pad_maximum_fusion), channel_id=1, source_target_pairs={{0,4},{4,8},{8,12},{12,16},{16,20},{20,24},{24,28},{1,5},{5,9},{9,... | collective-permute-start | bytes 835592 | tf_op jit(solution)/shard_map/ppermute | solution.py:25
  46.7 12.3 %collective-permute-done.1 = bf16[136,1024]{1,0:T(8,128)(2,1)S(1)} collective-permute-done((bf16[136,1024]{1,0:T(8,128)(2,1)S(1)}, bf16[136,1024]{1,0:T(8,128)(2,1)S(1)}, u32[]{:S(2)}, u32[]{:S(2)}) %collective-permute-start.1) | collective-permute-done | bytes 278560 | tf_op jit(solution)/shard_map/ppermute | solution.py:25
  59.0 1.1 fusion
  60.2 5.4 %collective-permute-start.2 = (bf16[136,1024]{1,0:T(8,128)(2,1)S(1)}, bf16[136,1024]{1,0:T(8,128)(2,1)S(1)}, u32[]{:S(2)}, u32[]{:S(2)}) collective-permute-start(bf16[136,1024]{1,0:T(8,128)(2,1)S(1)} %pad_maximum_fusion.1), channel_id=1, source_target_pairs={{0,8},{4,12},{8,16},{12,20},{16,24},{20,28},{1,9},{5,13},{9,17},{1... | collective-permute-start | bytes 835592 | tf_op jit(solution)/shard_map/ppermute | solution.py:25
  65.6 11.7 %collective-permute-done.2 = bf16[136,1024]{1,0:T(8,128)(2,1)S(1)} collective-permute-done((bf16[136,1024]{1,0:T(8,128)(2,1)S(1)}, bf16[136,1024]{1,0:T(8,128)(2,1)S(1)}, u32[]{:S(2)}, u32[]{:S(2)}) %collective-permute-start.2) | collective-permute-done | bytes 278560 | tf_op jit(solution)/shard_map/ppermute | solution.py:25
  77.5 5.6 %collective-permute-start.3 = (bf16[136,1024]{1,0:T(8,128)(2,1)S(1)}, bf16[136,1024]{1,0:T(8,128)(2,1)S(1)}, u32[]{:S(2)}, u32[]{:S(2)}) collective-permute-start(bf16[136,1024]{1,0:T(8,128)(2,1)S(1)} %pad_maximum_fusion.2), channel_id=1, source_target_pairs={{0,16},{4,20},{8,24},{12,28},{1,17},{5,21},{9,25},{13,29},{2,18},{... | collective-permute-start | bytes 835592 | tf_op jit(solution)/shard_map/ppermute | solution.py:25
  83.1 4.4 %collective-permute-done.3 = bf16[136,1024]{1,0:T(8,128)(2,1)S(1)} collective-permute-done((bf16[136,1024]{1,0:T(8,128)(2,1)S(1)}, bf16[136,1024]{1,0:T(8,128)(2,1)S(1)}, u32[]{:S(2)}, u32[]{:S(2)}) %collective-permute-start.3) | collective-permute-done | bytes 278560 | tf_op jit(solution)/shard_map/ppermute | solution.py:25
  87.7 14.5 %collective-permute-start.4 = (bf16[128,1024]{1,0:T(8,128)(2,1)S(1)}, bf16[128,1024]{1,0:T(8,128)(2,1)S(1)}, u32[]{:S(2)}, u32[]{:S(2)}) collective-permute-start(bf16[128,1024]{1,0:T(8,128)(2,1)S(1)} %add_convert_fusion), channel_id=1, source_target_pairs={{0,4},{4,8},{8,12},{12,16},{16,20},{20,24},{24,28},{1,5},{5,9},{9,... | collective-permute-start | bytes 786440 | tf_op jit(solution)/shard_map/ppermute | solution.py:25
  102.2 1.2 copy.35
  103.5 0.7 broadcast_in_dim_reshape.3.skip_ref
  104.2 9.0 %collective-permute-done.4 = bf16[128,1024]{1,0:T(8,128)(2,1)S(1)} collective-permute-done((bf16[128,1024]{1,0:T(8,128)(2,1)S(1)}, bf16[128,1024]{1,0:T(8,128)(2,1)S(1)}, u32[]{:S(2)}, u32[]{:S(2)}) %collective-permute-start.4) | collective-permute-done | bytes 262176 | tf_op jit(solution)/shard_map/ppermute | solution.py:25
  113.1 0.8 convert_element_type.37.enter_ref
  114.0 25.6 %mixer_output.1 = bf16[1536,1024]{1,0:T(8,128)(2,1)} custom-call(bf16[1536,1024]{1,0:T(8,128)(2,1)} %x_ref.5, bf16[8,1024]{1,0:T(8,128)(2,1)} %slice.48.xr_ref, bf16[4,1024]{1,0:T(4,128)(2,1)} %xt_ref.3, bf16[1536,256]{1,0:T(8,128)(2,1)} %b_ref.3, bf16[8,256]{1,0:T(8,128)(2,1)} %get-tuple-element.14.br_ref, bf16[4,256]{1,0:T(4,128)(2,1)} %bt_ref.3, ...), custom_call_target="tpu_custom_call" | custom-call | flops 4831838208 | bytes 37748736 | tf_op jit(solution)/shard_map/mixer_output/pallas_call | solution.py:237
  139.6 11.4 %convolution_convert_fusion.mix_ref = bf16[1536,2048]{1,0:T(8,128)(2,1)} fusion(bf16[1536,1024]{1,0:T(8,128)(2,1)} %mixer_output.1, bf16[1024,2048]{1,0:T(8,128)(2,1)} %param.34), kind=kOutput, calls=%fused_computation | convolution fusion | flops 6445596672 | bytes 13631488 | tf_op jit(solution)/shard_map/dot_general | solution.py:265
  151.0 128.5 %experts.1 = (bf16[128,2048]{1,0:T(8,128)(2,1)}, bf16[384,2048]{1,0:T(8,128)(2,1)}) custom-call(bf16[4096,2176]{1,0:T(8,128)(2,1)} %all-gather.2.cloned.1.call-done.tokens_ref, bf16[1536,2048]{1,0:T(8,128)(2,1)} %convolution_convert_fusion.mix_ref, bf16[2048,512]{1,0:T(8,128)(2,1)} %bitcast.40, bf16[2048,512]{1,0:T(8,128)(2,1)} %bitcast.41, ...), custom_call_target="tpu_custom_call" | custom-call | flops 128849018880 | bytes 35651584 | tf_op jit(solution)/shard_map/experts/pallas_call | solution.py:704
  279.6 2.8 copy.52
  282.3 0.8 copy.53
  (33 shorter events, 2.0 us)
Async XLA Ops:
  7.2 143.9 %all-gather.2.cloned.1.call-start = ((), (), s32[]{:S(2)}) async-start(), calls=%async_computation | async-start | bytes 18382848 | tf_op jit(solution)/shard_map/all_gather | solution.py:689
  14.7 10.0 %collective-permute-start = (bf16[8,1536]{1,0:T(8,128)(2,1)S(1)}, bf16[8,1536]{1,0:T(8,128)(2,1)S(1)}, u32[]{:S(2)}, u32[]{:S(2)}) collective-permute-start(bf16[8,1536]{1,0:T(8,128)(2,1)S(1)} %pad_maximum_fusion.3), channel_id=1, source_target_pairs={{0,4},{4,8},{8,12},{12,16},{16,20},{20,24},{24,28},{1,5},{5,9},{9,... | collective-permute-start | bytes 73736 | tf_op jit(solution)/shard_map/ppermute | solution.py:25
  41.9 35.4 %copy-start = (f32[128,1024]{1,0:T(8,128)S(1)}, f32[128,1024]{1,0:T(8,128)}, u32[]{:S(2)}) copy-start(f32[128,1024]{1,0:T(8,128)} %own_state.1) | copy-start | bytes 1572868
  43.1 60.3 %copy-start.2 = (f32[16]{0:T(128)S(1)}, f32[16]{0:T(128)}, u32[]{:S(2)}) copy-start(f32[16]{0:T(128)} %param.31) | copy-start | bytes 196
  43.1 15.9 %collective-permute-start.1 = (bf16[136,1024]{1,0:T(8,128)(2,1)S(1)}, bf16[136,1024]{1,0:T(8,128)(2,1)S(1)}, u32[]{:S(2)}, u32[]{:S(2)}) collective-permute-start(bf16[136,1024]{1,0:T(8,128)(2,1)S(1)} %pad_maximum_fusion), channel_id=1, source_target_pairs={{0,4},{4,8},{8,12},{12,16},{16,20},{20,24},{24,28},{1,5},{5,9},{9,... | collective-permute-start | bytes 835592 | tf_op jit(solution)/shard_map/ppermute | solution.py:25
  60.2 17.1 %collective-permute-start.2 = (bf16[136,1024]{1,0:T(8,128)(2,1)S(1)}, bf16[136,1024]{1,0:T(8,128)(2,1)S(1)}, u32[]{:S(2)}, u32[]{:S(2)}) collective-permute-start(bf16[136,1024]{1,0:T(8,128)(2,1)S(1)} %pad_maximum_fusion.1), channel_id=1, source_target_pairs={{0,8},{4,12},{8,16},{12,20},{16,24},{20,28},{1,9},{5,13},{9,17},{1... | collective-permute-start | bytes 835592 | tf_op jit(solution)/shard_map/ppermute | solution.py:25
  77.5 10.0 %collective-permute-start.3 = (bf16[136,1024]{1,0:T(8,128)(2,1)S(1)}, bf16[136,1024]{1,0:T(8,128)(2,1)S(1)}, u32[]{:S(2)}, u32[]{:S(2)}) collective-permute-start(bf16[136,1024]{1,0:T(8,128)(2,1)S(1)} %pad_maximum_fusion.2), channel_id=1, source_target_pairs={{0,16},{4,20},{8,24},{12,28},{1,17},{5,21},{9,25},{13,29},{2,18},{... | collective-permute-start | bytes 835592 | tf_op jit(solution)/shard_map/ppermute | solution.py:25
  87.7 25.4 %collective-permute-start.4 = (bf16[128,1024]{1,0:T(8,128)(2,1)S(1)}, bf16[128,1024]{1,0:T(8,128)(2,1)S(1)}, u32[]{:S(2)}, u32[]{:S(2)}) collective-permute-start(bf16[128,1024]{1,0:T(8,128)(2,1)S(1)} %add_convert_fusion), channel_id=1, source_target_pairs={{0,4},{4,8},{8,12},{12,16},{16,20},{20,24},{24,28},{1,5},{5,9},{9,... | collective-permute-start | bytes 786440 | tf_op jit(solution)/shard_map/ppermute | solution.py:25
  279.5 2.8 copy-start.1
Sparse Core Ops, SparseCore 0:
  12.7 132.1 all-gather.1

commit v3 on v2

--- a/solution.py
+++ b/solution.py
@@ -164,6 +164,7 @@
     spike_fading_exponent,
     cluster_scaling_vector,
     sequence_exit_projection,
+    marked,
 ):
     tok_rows = sequence_entry_features.shape[0]
     local_heads = interval_offset.shape[0]
@@ -220,6 +221,13 @@
     x_args = (sequence_entry_features, rim_x, entry_filter_taps)
     b_args = (memory_insert_clusters, rim_b, insert_filter_taps)
     c_args = (memory_query_clusters, rim_c, query_filter_taps)
+    if marked is not None:
+        return mixer_gather(
+            per_group, local_groups, blocks, x_args, b_args, c_args, sequence_exit_gating, key_log,
+            cumulative, row_log, end_factor, own_decay,
+            jnp.repeat(skip_connection_factor, HEAD)[None], cluster_scaling_vector[None],
+            sequence_exit_projection, marked,
+        )
     own_state = pl.pallas_call(
         functools.partial(state_kernel, per_group, local_groups),
         grid=(blocks,),
@@ -264,6 +272,99 @@
     )
     return jnp.dot(normed, sequence_exit_projection, preferred_element_type=jnp.float32).astype(
         jnp.bfloat16
+    )
+
+
+def mixer_gather(
+    per_group, groups, blocks, x_args, b_args, c_args, gating, key_log, cumulative, row_log,
+    end_factor, own_decay, skip, scale, exit_projection, marked,
+):
+    tok_rows, inner_cols = gating.shape
+    state_cols = b_args[0].shape[1]
+    heads = key_log.shape[1]
+    features = exit_projection.shape[1]
+    rows, marked_cols = marked.shape
+    taps = x_args[2].shape[0]
+    devices = lax.axis_size("ep") * lax.axis_size("tp")
+    depth = lax.axis_size("ep") // 2
+    narrow, wide = jnp.bfloat16, inner_cols // 2
+    pieces = 7 * depth
+
+    def either(i):
+        return jnp.where(i < blocks, i, jnp.maximum(i - blocks - 1, 0))
+
+    def late(i):
+        return jnp.maximum(i - blocks - 1, 0)
+
+    def by_rows(width, at):
+        return pl.BlockSpec((SPAN, width), lambda i: (at(i), 0))
+
+    def by_block(count, width, at):
+        return pl.BlockSpec((1, count, width), lambda i: (at(i), 0, 0))
+
+    def fixed(shape):
+        return pl.BlockSpec(shape, lambda i: (0, 0))
+
+    def conv_specs(width, at):
+        return [by_rows(width, at), fixed((RIM, width)), fixed((taps, width))]
+
+    dma = pltpu.SemaphoreType.DMA
+    hops = [dma((depth,)) for _ in range(12)]
+    return pl.pallas_call(
+        functools.partial(mixer_gather_kernel, per_group, groups, blocks, depth),
+        grid=(2 * blocks + 1,),
+        in_specs=conv_specs(inner_cols, either)
+        + conv_specs(state_cols, either)
+        + conv_specs(state_cols, late)
+        + [
+            by_rows(inner_cols, late),
+            by_rows(heads, either),
+            by_rows(heads, late),
+            by_block(heads, SPAN, late),
+            by_block(1, inner_cols, either),
+            fixed((1, inner_cols)),
+            fixed((1, inner_cols)),
+            fixed((1, inner_cols)),
+            fixed((inner_cols, features)),
+            fixed((rows, marked_cols)),
+        ],
+        out_specs=[by_rows(features, late), pl.BlockSpec(memory_space=pl.ANY)],
+        out_shape=[
+            jax.ShapeDtypeStruct((tok_rows, features), narrow),
+            jax.ShapeDtypeStruct((devices * rows, marked_cols), narrow),
+        ],
+        scratch_shapes=[
+            pltpu.VMEM((SPAN + RIM, inner_cols), jnp.float32),
+            pltpu.VMEM((SPAN + RIM, state_cols), jnp.float32),
+            pltpu.VMEM((SPAN + RIM, state_cols), jnp.float32),
+            pltpu.VMEM((STATE, inner_cols), jnp.float32),
+            pltpu.VMEM((SPAN, inner_cols), jnp.float32),
+            pltpu.VMEM((SPAN, inner_cols), narrow),
+            pltpu.VMEM((STATE + 2 * RIM, inner_cols), narrow),
+            pltpu.VMEM((STATE + 2 * RIM, inner_cols), narrow),
+            pltpu.VMEM((STATE + 2 * RIM, wide), narrow),
+            pltpu.VMEM((depth - 1, STATE + 2 * RIM, wide), narrow),
+            pltpu.VMEM((STATE, wide), jnp.float32),
+            pltpu.VMEM((STATE, wide), narrow),
+            pltpu.VMEM((STATE, wide), narrow),
+            dma((1,)), dma((depth - 1,)), dma((depth - 1,)),
+            *hops,
+            dma((pieces,)), dma((pieces,)), dma((1,)), dma((1,)), dma((depth - 1,)),
+            dma((depth - 1,)), dma((1,)), dma((1,)),
+        ],
+        compiler_params=pltpu.CompilerParams(
+            collective_id=1, has_side_effects=True, vmem_limit_bytes=56 * 1024 * 1024,
+            dimension_semantics=("arbitrary",),
+        ),
+        cost_estimate=pl.CostEstimate(
+            flops=tok_rows * inner_cols * (features * 2 + STATE * 16),
+            bytes_accessed=tok_rows * inner_cols * 16,
+            transcendentals=0,
+        ),
+        name="mixer_gather",
+    )(
+        *x_args, *b_args, *c_args, gating, key_log, cumulative, row_log, end_factor, own_decay,
+        skip, scale, exit_projection, marked,
     )
 
 
@@ -668,17 +769,318 @@
         z_copy(i).wait_send()
 
 
+def mixer_gather_kernel(
+    per_group, groups, blocks, depth,
+    x_ref, xr_ref, xt_ref, b_ref, br_ref, bt_ref, c_ref, cr_ref, ct_ref, z_ref, lw_ref, cum_ref,
+    row_ref, end_ref, decay_ref, skip_ref, scale_ref, exit_ref, marked_ref,
+    part_ref, tokens_ref,
+    xbuf, bbuf, cbuf, state, ybuf, nbuf, pair_out, pair_in, line_out, line_in, line_sum, swap_out,
+    swap_in, local_sem, z_send, z_recv, xa_s, xa_r, xb_s, xb_r, xf_s, xf_r, ya_s, ya_r, yb_s, yb_r,
+    yf_s, yf_r, d_s, d_r, pair_s, pair_r, line_s, line_r, swap_s, swap_r,
+):
+    step = pl.program_id(0)
+    ep, tp = lax.axis_index("ep"), lax.axis_index("tp")
+    z, y, x, core = ep // 2, ep % 2, tp // 2, tp % 2
+    sibling = {"tp": x * 2 + 1 - core}
+    x_next = {"tp": (1 - x) * 2 + core}
+    y_next = {"ep": z * 2 + 1 - y}
+    mesh_id = pl.DeviceIdType.MESH
+    rows = marked_ref.shape[0]
+    part_rows = rows // 2
+    inner = state.shape[1]
+    wide = inner // 2
+
+    def z_next(k):
+        return {"ep": ((z + k) % depth) * 2 + y}
+
+    def remote(source, target, send, recv, device):
+        return pltpu.make_async_remote_copy(
+            src_ref=source, dst_ref=target, send_sem=send, recv_sem=recv,
+            device_id=device, device_id_type=mesh_id,
+        )
+
+    def region(dx, dy, k, half, c=core):
+        block = (((z + depth - k) % depth) * 2 + (y + dy) % 2) * 4 + ((x + dx) % 2) * 2 + c
+        size = rows if half is None else part_rows
+        start = block * rows + (0 if half is None else half * part_rows)
+        return tokens_ref.at[pl.ds(pl.multiple_of(start, part_rows), size)]
+
+    def source(dx, dy, k, half):
+        if (dx, dy, k) == (0, 0, 0):
+            if half is None:
+                return marked_ref
+            return marked_ref.at[pl.ds(half * part_rows, part_rows)]
+        return region(dx, dy, k, half)
+
+    def z_copy(k):
+        return remote(
+            marked_ref, region(0, 0, 0, None), z_send.at[k - 1], z_recv.at[k - 1], z_next(k)
+        )
+
+    def z_came(k):
+        here = region(0, 0, k, None)
+        return remote(here, here, z_send.at[k - 1], z_recv.at[k - 1], z_next(k))
+
+    moves = {
+        "xa": ((0, 0, 0), (1, 0, 0), xa_s, xa_r, x_next),
+        "xb": ((0, 0, 1), (1, 0, 1), xb_s, xb_r, x_next),
+        "xf": ((0, 1, 1), (1, 1, 1), xf_s, xf_r, x_next),
+        "yb": ((0, 0, 1), (0, 1, 1), yb_s, yb_r, y_next),
+        "ya": ((0, 0, 0), (0, 1, 0), ya_s, ya_r, y_next),
+        "yf": ((1, 0, 0), (1, 1, 0), yf_s, yf_r, y_next),
+    }
+
+    def sent(name, k):
+        (dx, dy, half), _, send, recv, device = moves[name]
+        return remote(
+            source(dx, dy, k, half), region(dx, dy, k, half), send.at[k], recv.at[k], device
+        )
+
+    def came(name, k):
+        _, (dx, dy, half), send, recv, device = moves[name]
+        here = region(dx, dy, k, half)
+        return remote(here, here, send.at[k], recv.at[k], device)
+
+    shared = [(0, 0, None), (1, 0, 0), (1, 0, 1), (0, 1, 1), (0, 1, 0), (1, 1, 0), (1, 1, 1)]
+
+    def d_sent(k, n):
+        dx, dy, half = shared[n]
+        m = len(shared) * k + n
+        return remote(
+            source(dx, dy, k, half), region(dx, dy, k, half), d_s.at[m], d_r.at[m], sibling
+        )
+
+    def d_came(k, n):
+        dx, dy, half = shared[n]
+        m = len(shared) * k + n
+        here = region(dx, dy, k, half, 1 - core)
+        return remote(here, here, d_s.at[m], d_r.at[m], sibling)
+
+    def first_hop(k):
+        if k > 0:
+            z_came(k).wait_recv()
+        for name in ("xa", "yb", "xb", "ya"):
+            sent(name, k).start()
+        d_sent(k, 0).start()
+
+    def second_hop(k):
+        came("xa", k).wait_recv()
+        sent("yf", k).start()
+        d_sent(k, 1).start()
+        came("yb", k).wait_recv()
+        sent("xf", k).start()
+        d_sent(k, 3).start()
+
+    def last_hop(k, parts=(("xb", 2), ("ya", 4), ("yf", 5), ("xf", 6))):
+        for name, n in parts:
+            came(name, k).wait_recv()
+            d_sent(k, n).start()
+
+    def own_copy():
+        return pltpu.make_async_copy(marked_ref, region(0, 0, 0, None), local_sem.at[0])
+
+    @pl.when(step == 0)
+    def _():
+        barrier = pltpu.get_barrier_semaphore()
+        partners = [sibling, x_next, y_next] + [z_next(k) for k in range(1, depth)]
+        for partner in partners:
+            pl.semaphore_signal(barrier, inc=1, device_id=partner, device_id_type=mesh_id)
+        pl.semaphore_wait(barrier, len(partners))
+        z_copy(1).start()
+        first_hop(0)
+        for k in range(2, depth - 1):
+            z_copy(k).start()
+        own_copy().start()
+
+    low = lax.broadcasted_iota(jnp.int32, (SPAN, 2 * HEAD), 1) < HEAD
+    state_pass = step < blocks
+    output_pass = step > blocks
+
+    @pl.when(state_pass)
+    def _():
+        first = step == 0
+        xv = conv_block(xbuf, first, x_ref, xr_ref, xt_ref)
+        bv = conv_block(bbuf, first, b_ref, br_ref, bt_ref)
+
+        @pl.when(first)
+        def _():
+            state[...] = jnp.zeros_like(state)
+
+        lw = lw_ref[...]
+        for g in range(groups):
+            bt = bv[:, g * STATE : (g + 1) * STATE].T.astype(jnp.bfloat16)
+            for pair in range(per_group // 2):
+                h = g * per_group + 2 * pair
+                cols = slice(h * HEAD, (h + 2) * HEAD)
+                factor = jnp.exp(
+                    jnp.where(low, spread(lw, h, 2 * HEAD), spread(lw, h + 1, 2 * HEAD))
+                )
+                xw = (xv[:, cols] * factor).astype(jnp.bfloat16)
+                added = jnp.dot(bt, xw, preferred_element_type=jnp.float32)
+                state[:, cols] = state[:, cols] * end_ref[0, :, cols] + added
+
+    @pl.when(step == blocks // 2)
+    def _():
+        second_hop(0)
+
+    @pl.when(step == blocks)
+    def _():
+        pair = remote(pair_out, pair_in, pair_s.at[0], pair_r.at[0], y_next)
+        swap = remote(swap_out, swap_in, swap_s.at[0], swap_r.at[0], y_next)
+
+        def line(k):
+            return remote(
+                line_out, line_in.at[k - 1], line_s.at[k - 1], line_r.at[k - 1], z_next(k)
+            )
+
+        decay = decay_ref[...]
+        pair_out[:STATE, :] = state[...].astype(jnp.bfloat16)
+        pair_out[STATE:, :] = jnp.broadcast_to(decay, (2 * RIM, inner)).astype(jnp.bfloat16)
+        last_hop(0, (("xb", 2), ("ya", 4)))
+        pair.start()
+        first_hop(1)
+        last_hop(0, (("yf", 5), ("xf", 6)))
+        pair.wait_recv()
+        mine = pl.ds(pl.multiple_of(y * wide, wide), wide)
+        theirs = pl.ds(pl.multiple_of((1 - y) * wide, wide), wide)
+        own_state, own_decay = state[:, mine], decay_ref[:, mine]
+        other_state = pair_in[:STATE, mine].astype(jnp.float32)
+        other_decay = pair_in[STATE : STATE + 1, mine].astype(jnp.float32)
+        later = y == 1
+        both = jnp.where(
+            later, other_state * own_decay + own_state, own_state * other_decay + other_state
+        )
+        line_out[:STATE, :] = both.astype(jnp.bfloat16)
+        line_out[STATE:, :] = jnp.broadcast_to(own_decay * other_decay, (2 * RIM, wide)).astype(
+            jnp.bfloat16
+        )
+        line_sum[...] = jnp.zeros_like(line_sum)
+        for k in range(1, depth):
+            @pl.when(z + k < depth)
+            def _():
+                line(k).start()
+
+        z_copy(depth - 1).start()
+        for k in range(depth - 1, 0, -1):
+            @pl.when(z >= k)
+            def _():
+                line(k).wait_recv()
+                line_sum[...] = line_sum[...] * line_in[k - 1, STATE : STATE + 1, :].astype(
+                    jnp.float32
+                ) + line_in[k - 1, :STATE, :].astype(jnp.float32)
+
+        swap_out[...] = line_sum[...].astype(jnp.bfloat16)
+        state[:, mine] = line_sum[...]
+        second_hop(1)
+        swap.start()
+        swap.wait_recv()
+        state[:, theirs] = swap_in[...].astype(jnp.float32)
+
+        @pl.when(later)
+        def _():
+            state[...] = state[...] * pair_in[STATE : STATE + 1, :].astype(jnp.float32) + pair_in[
+                :STATE, :
+            ].astype(jnp.float32)
+
+        pair.wait_send()
+        swap.wait_send()
+        for k in range(1, depth):
+            @pl.when(z + k < depth)
+            def _():
+                line(k).wait_send()
+
+    @pl.when(output_pass)
+    def _():
+        first = step == blocks + 1
+        xv = conv_block(xbuf, first, x_ref, xr_ref, xt_ref)
+        bv = conv_block(bbuf, first, b_ref, br_ref, bt_ref)
+        cv = conv_block(cbuf, first, c_ref, cr_ref, ct_ref)
+        lw = lw_ref[...]
+        cum = cum_ref[...]
+        causal = lax.broadcasted_iota(jnp.int32, (SPAN, SPAN), 0) >= lax.broadcasted_iota(
+            jnp.int32, (SPAN, SPAN), 1
+        )
+        group_cols = per_group * HEAD
+        for g in range(groups):
+            bt = bv[:, g * STATE : (g + 1) * STATE].T.astype(jnp.bfloat16)
+            cg = cv[:, g * STATE : (g + 1) * STATE].astype(jnp.bfloat16)
+            scores = jnp.dot(cg, bt, preferred_element_type=jnp.float32)
+            squares = jnp.zeros((SPAN, 2 * HEAD), jnp.float32)
+            for pair in range(per_group // 2):
+                h = g * per_group + 2 * pair
+                cols = slice(h * HEAD, (h + 2) * HEAD)
+                xp = xv[:, cols]
+                cum_0, cum_1 = spread(cum, h, SPAN), spread(cum, h + 1, SPAN)
+                row_0, row_1 = row_ref[0, h : h + 1, :], row_ref[0, h + 1 : h + 2, :]
+                m_0 = scores * jnp.exp(jnp.where(causal, cum_0 + row_0, -jnp.inf))
+                m_1 = scores * jnp.exp(jnp.where(causal, cum_1 + row_1, -jnp.inf))
+                mixing = jnp.concatenate([m_0.astype(jnp.bfloat16), m_1.astype(jnp.bfloat16)], axis=1)
+                x_0 = jnp.where(low, xp, 0.0).astype(jnp.bfloat16)
+                x_1 = jnp.where(low, 0.0, xp).astype(jnp.bfloat16)
+                value = jnp.dot(
+                    mixing, jnp.concatenate([x_0, x_1], axis=0), preferred_element_type=jnp.float32
+                )
+                before = state[:, cols]
+                carried = jnp.dot(cg, before.astype(jnp.bfloat16), preferred_element_type=jnp.float32)
+                value = value + carried * jnp.exp(jnp.where(low, cum_0, cum_1)) + xp * skip_ref[:, cols]
+                factor = jnp.exp(
+                    jnp.where(low, spread(lw, h, 2 * HEAD), spread(lw, h + 1, 2 * HEAD))
+                )
+                xw = (xp * factor).astype(jnp.bfloat16)
+                added = jnp.dot(bt, xw, preferred_element_type=jnp.float32)
+                state[:, cols] = before * end_ref[0, :, cols] + added
+                gate = z_ref[:, cols].astype(jnp.float32)
+                gated = value * (gate * jax.nn.sigmoid(gate))
+                squares = squares + gated * gated
+                ybuf[:, cols] = gated
+            mean = jnp.sum(squares, axis=1, keepdims=True) / group_cols
+            inverse = lax.rsqrt(mean + norm_eps)
+            cols = slice(g * group_cols, (g + 1) * group_cols)
+            nbuf[:, cols] = (ybuf[:, cols] * inverse * scale_ref[:, cols]).astype(jnp.bfloat16)
+        part_ref[...] = jnp.dot(
+            nbuf[...], exit_ref[...], preferred_element_type=jnp.float32
+        ).astype(jnp.bfloat16)
+
+    pace = blocks // (2 * depth - 2)
+    for k in range(2, depth):
+        at = blocks + 1 + (2 * k - 3) * pace
+
+        @pl.when(step == at)
+        def _():
+            first_hop(k)
+
+        @pl.when(step == at + pace)
+        def _():
+            second_hop(k)
+            last_hop(k - 1)
+
+    @pl.when(step == 2 * blocks)
+    def _():
+        last_hop(depth - 1)
+        for k in range(depth):
+            for n in range(len(shared)):
+                d_came(k, n).wait_recv()
+        own_copy().wait()
+        for k in range(1, depth):
+            z_copy(k).wait_send()
+        for k in range(depth):
+            for name in moves:
+                sent(name, k).wait_send()
+            for n in range(len(shared)):
+                d_sent(k, n).wait_send()
+
+
 def dense_experts_fit(tok_rows, top_count, capacity, mix_rows):
     experts = lax.axis_size("ep")
     fits = experts % 2 == 0 and experts >= 4 and 3 * experts <= LANES and lax.axis_size("tp") == 4
     return fits and 2 * top_count >= experts and mix_rows % (4 * MIX_ROWS) == 0 and tok_rows == LANES and capacity % 16 == 0
 
 
-def gathered_tokens(
+def marked_tokens(
     specialist_sample_slice, specialist_scaling_vector, chosen_specialists, dispatcher_affinity_matrix
 ):
     rows, features = specialist_sample_slice.shape
-    marked = pl.pallas_call(
+    return pl.pallas_call(
         functools.partial(routing_kernel, lax.axis_size("ep")),
         out_shape=jax.ShapeDtypeStruct((rows, features + LANES), jnp.bfloat16),
         name="routing",
@@ -686,7 +1088,6 @@
         specialist_sample_slice, specialist_scaling_vector[None], chosen_specialists,
         dispatcher_affinity_matrix,
     )
-    return lax.all_gather(marked, ("ep", "tp"), axis=0, tiled=True)
 
 
 def experts_dense(
@@ -773,8 +1174,9 @@
     tok_rows, top_count = chosen_specialists.shape
     capacity = tok_rows * top_count * 5 // (4 * lax.axis_size("ep"))
     dense = dense_experts_fit(tok_rows, top_count, capacity, sequence_entry_features.shape[0])
+    marked = None
     if dense:
-        tokens = gathered_tokens(
+        marked = marked_tokens(
             specialist_sample_slice,
             specialist_scaling_vector,
             chosen_specialists,
@@ -795,8 +1197,10 @@
         spike_fading_exponent,
         cluster_scaling_vector,
         sequence_exit_projection,
+        marked,
     )
     if dense:
+        mix_part, tokens = mix_part
         moe_out, mixed = experts_dense(
             tokens, mix_part, tok_rows, capacity, gating_projection, expand_projection, shrink_projection
         )

time: 291 us -> 254 us (0.87)
  Pallas kernels: 173 us -> 230 us
  waiting for transfers between devices: 37.5 us -> 0.01 us
  starting transfers between devices: 33.8 us -> 4.89 us
  between operations: 14.2 us -> 0.69 us
  matrix products: 11.7 us -> 0.28 us
  other arithmetic: 5.54 us -> 2.01 us
    pallas_call x3 -> x2, Pallas kernels: 44.2 us -> 104 us  [the longest x1 101 us: mixer_gather(): pl.pallas_call(functools.partial(mixer_gather_kernel, per_group, groups,...]
    ppermute x5 -> x1, waiting for transfers between devices: 37.5 us -> 0.01 us  [passed_along(): return lax.ppermute(block, axis, route)]
    ppermute x5 -> x1, starting transfers between devices: 33.8 us -> 4.89 us  [passed_along(): return lax.ppermute(block, axis, route)]
    dot_general x1 -> x0, matrix products: 11.4 us -> none  [mixer_half(): jnp.dot(normed, sequence_exit_projection, preferred_element_type=jnp.floa...]
    unnamed x10 -> x6, local copies, waits for them, and re-layouts: 6.42 us -> 6.39 us
  transfers between devices with their start and end apart: 6 -> 1, of which waited for: 4 -> 0; matrix products, arithmetic and copies ran while one was open for 9% -> 4% of each run, Pallas kernels for 14% -> 1%
where the time goes in v3:
time: 254 us; the launch traced here: 253 us
  Pallas kernels  230 us (91%)
  local copies, waits for them, and re-layouts  15.6 us (6%)
  starting transfers between devices  4.89 us (2%)
    pallas_call x1, Pallas kernels, experts_dense(): pl.pallas_call(functools.partial(experts_kernel, experts, capacity), in_s...  126 us
    pallas_call x1, Pallas kernels, mixer_gather(): pl.pallas_call(functools.partial(mixer_gather_kernel, per_group, groups,...  101 us
    unnamed x6, local copies, waits for them, and re-layouts  6.39 us
  transfers between devices with their start and end apart: 1, of which 0 were waited for; matrix products, arithmetic and copies ran while one was open for 4% of the time, Pallas kernels for 1%

profile of v3, /device:TPU:0, one launch (start us, length us, event | category | flops | bytes accessed | tf_op | source)
XLA Modules:
  0.0 253.5 jit_solution(14955666122178316879)
XLA Ops:
  0.6 0.7 slice.22
  1.3 0.7 slice.23
  2.0 0.7 slice.21
  2.7 4.9 %collective-permute-start = (bf16[8,1536]{1,0:T(8,128)(2,1)S(1)}, bf16[8,1536]{1,0:T(8,128)(2,1)S(1)}, u32[]{:S(2)}, u32[]{:S(2)}) collective-permute-start(bf16[8,1536]{1,0:T(8,128)(2,1)S(1)} %pad_maximum_fusion), channel_id=1, source_target_pairs={{0,4},{4,8},{8,12},{12,16},{16,20},{20,24},{24,28},{1,5},{5,9},{9,... | collective-permute-start | bytes 73736 | tf_op jit(solution)/shard_map/ppermute | solution.py:25
  7.6 0.7 exp.19
  8.3 1.1 log_bitcast_fusion
  9.4 0.3 convolution_bitcast_fusion
  9.7 0.2 slice_reduce_fusion
  9.9 0.7 fusion.4
  10.6 1.1 copy.35
  11.7 0.7 broadcast_in_dim.34
  12.4 0.7 broadcast_in_dim_reshape.3.skip_ref
  13.1 1.4 copy.30.chosen_ref
  14.5 1.4 copy.31.score_ref
  15.9 0.1 broadcast_in_dim.32
  16.0 0.7 broadcast_in_dim.33.decay_ref
  16.7 0.1 broadcast_in_dim.30
  16.8 0.7 broadcast_in_dim.31.end_ref
  17.5 1.2 copy.34
  18.6 2.5 routing.1.marked_ref
  21.2 0.0 collective-permute-done
  21.2 0.6 fusion.9
  21.8 0.6 slice.28.xr_ref
  22.4 101.5 %mixer_gather.1 = (bf16[1536,2048]{1,0:T(8,128)(2,1)}, bf16[4096,2176]{1,0:T(8,128)(2,1)}) custom-call(bf16[1536,1024]{1,0:T(8,128)(2,1)} %x_ref.3, bf16[8,1024]{1,0:T(8,128)(2,1)} %slice.28.xr_ref, bf16[4,1024]{1,0:T(4,128)(2,1)} %xt_ref.1, bf16[1536,256]{1,0:T(8,128)(2,1)} %b_ref.1, bf16[8,256]{1,0:T(8,128)(2,1)} %get-tuple-element.18.br_ref, ...), custom_call_target="tpu_custom_call" | custom-call | flops 9663676416 | bytes 25165824 | tf_op jit(solution)/shard_map/mixer_gather/pallas_call | solution.py:313
  123.8 126.1 %experts.1 = (bf16[128,2048]{1,0:T(8,128)(2,1)}, bf16[384,2048]{1,0:T(8,128)(2,1)}) custom-call(bf16[4096,2176]{1,0:T(8,128)(2,1)} %get-tuple-element.6.tokens_ref, bf16[1536,2048]{1,0:T(8,128)(2,1)} %get-tuple-element.7.mix_ref, bf16[2048,512]{1,0:T(8,128)(2,1)} %bitcast.30, bf16[2048,512]{1,0:T(8,128)(2,1)} %bitcast.31, bf16[512,2048]{1,0:T(8,128)(2,1)} %bitcast.32), custom_call_target="tpu_custom_call" | custom-call | flops 128849018880 | bytes 35651584 | tf_op jit(solution)/shard_map/experts/pallas_call | solution.py:1105
  249.9 0.0 copy-start
  249.9 2.8 %copy.51 = bf16[384,2048]{1,0:T(8,128)(2,1)} copy(bf16[384,2048]{1,0:T(8,128)(2,1)} %get-tuple-element.21) | data formatting | bytes 3145728
  252.7 0.0 copy-done
  252.7 0.8 copy.52
  (2 shorter events, 0.0 us)
Async XLA Ops:
  2.7 18.4 %collective-permute-start = (bf16[8,1536]{1,0:T(8,128)(2,1)S(1)}, bf16[8,1536]{1,0:T(8,128)(2,1)S(1)}, u32[]{:S(2)}, u32[]{:S(2)}) collective-permute-start(bf16[8,1536]{1,0:T(8,128)(2,1)S(1)} %pad_maximum_fusion), channel_id=1, source_target_pairs={{0,4},{4,8},{8,12},{12,16},{16,20},{20,24},{24,28},{1,5},{5,9},{9,... | collective-permute-start | bytes 73736 | tf_op jit(solution)/shard_map/ppermute | solution.py:25
  249.9 2.8 %copy-start = (bf16[128,2048]{1,0:T(8,128)(2,1)S(1)}, bf16[128,2048]{1,0:T(8,128)(2,1)}, u32[]{:S(2)}) copy-start(bf16[128,2048]{1,0:T(8,128)(2,1)} %get-tuple-element.22) | copy-start | bytes 1572868

commit v4 on v3

--- a/solution.py
+++ b/solution.py
@@ -12,6 +12,7 @@
 RIM = 8
 LANES = 128
 MIX_ROWS = 32
+CUT_EIGHTHS = 5
 
 norm_eps = 1e-05
 clamp_top = 7.0
@@ -29,6 +30,26 @@
     @pl.when(first)
     def _():
         buf[0:RIM, :] = rim_ref[...].astype(jnp.float32)
+
+    @pl.when(jnp.logical_not(first))
+    def _():
+        buf[0:RIM, :] = buf[SPAN : SPAN + RIM, :]
+
+    buf[RIM : RIM + SPAN, :] = value_ref[...].astype(jnp.float32)
+    taps = taps_ref[...].astype(jnp.float32)
+    count = taps.shape[0]
+    total = buf[RIM : RIM + SPAN, :] * taps[count - 1 : count]
+    for j in range(count - 1):
+        start = RIM - (count - 1) + j
+        total = total + buf[start : start + SPAN, :] * taps[j : j + 1]
+    return total * jax.nn.sigmoid(total)
+
+
+def conv_after(buf, first, value_ref, rim_ref, has_rim, taps_ref):
+    @pl.when(first)
+    def _():
+        rim = rim_ref[...].astype(jnp.float32)[RIM:]
+        buf[0:RIM, :] = jnp.where(has_rim, rim, 0.0)
 
     @pl.when(jnp.logical_not(first))
     def _():
@@ -170,6 +191,16 @@
     local_heads = interval_offset.shape[0]
     local_groups = memory_insert_clusters.shape[1] // STATE
     per_group = local_heads // local_groups
+    if marked is not None:
+        heads = jnp.stack([interval_offset, head_fading_exponent, skip_connection_factor], axis=1)
+        return mixer_gather(
+            per_group, local_groups, tok_rows // SPAN,
+            (sequence_entry_features, memory_insert_clusters, memory_query_clusters),
+            (entry_filter_taps, insert_filter_taps, query_filter_taps), sequence_exit_gating,
+            interval_presoftplus.T, spike_fading_exponent.T,
+            jnp.pad(heads, ((0, 0), (0, LANES - heads.shape[1]))), cluster_scaling_vector[None],
+            sequence_exit_projection, marked,
+        )
     inner_cols = sequence_entry_features.shape[1]
     state_cols = memory_insert_clusters.shape[1]
     last_rows = jnp.concatenate(
@@ -221,13 +252,6 @@
     x_args = (sequence_entry_features, rim_x, entry_filter_taps)
     b_args = (memory_insert_clusters, rim_b, insert_filter_taps)
     c_args = (memory_query_clusters, rim_c, query_filter_taps)
-    if marked is not None:
-        return mixer_gather(
-            per_group, local_groups, blocks, x_args, b_args, c_args, sequence_exit_gating, key_log,
-            cumulative, row_log, end_factor, own_decay,
-            jnp.repeat(skip_connection_factor, HEAD)[None], cluster_scaling_vector[None],
-            sequence_exit_projection, marked,
-        )
     own_state = pl.pallas_call(
         functools.partial(state_kernel, per_group, local_groups),
         grid=(blocks,),
@@ -276,15 +300,15 @@
 
 
 def mixer_gather(
-    per_group, groups, blocks, x_args, b_args, c_args, gating, key_log, cumulative, row_log,
-    end_factor, own_decay, skip, scale, exit_projection, marked,
+    per_group, groups, blocks, streams, filters, gating, raw, spikes, heads, scale,
+    exit_projection, marked,
 ):
     tok_rows, inner_cols = gating.shape
-    state_cols = b_args[0].shape[1]
-    heads = key_log.shape[1]
+    state_cols = streams[1].shape[1]
+    head_count = raw.shape[0]
     features = exit_projection.shape[1]
     rows, marked_cols = marked.shape
-    taps = x_args[2].shape[0]
+    taps = filters[0].shape[0]
     devices = lax.axis_size("ep") * lax.axis_size("tp")
     depth = lax.axis_size("ep") // 2
     narrow, wide = jnp.bfloat16, inner_cols // 2
@@ -299,14 +323,17 @@
     def by_rows(width, at):
         return pl.BlockSpec((SPAN, width), lambda i: (at(i), 0))
 
-    def by_block(count, width, at):
-        return pl.BlockSpec((1, count, width), lambda i: (at(i), 0, 0))
+    def by_lanes(at):
+        return pl.BlockSpec((head_count, SPAN), lambda i: (0, at(i)))
+
+    def early(i):
+        return jnp.minimum(i, blocks - 1)
 
     def fixed(shape):
         return pl.BlockSpec(shape, lambda i: (0, 0))
 
     def conv_specs(width, at):
-        return [by_rows(width, at), fixed((RIM, width)), fixed((taps, width))]
+        return [by_rows(width, at), fixed((taps, width))]
 
     dma = pltpu.SemaphoreType.DMA
     hops = [dma((depth,)) for _ in range(12)]
@@ -318,22 +345,31 @@
         + conv_specs(state_cols, late)
         + [
             by_rows(inner_cols, late),
-            by_rows(heads, either),
-            by_rows(heads, late),
-            by_block(heads, SPAN, late),
-            by_block(1, inner_cols, either),
-            fixed((1, inner_cols)),
-            fixed((1, inner_cols)),
+            by_lanes(early),
+            by_lanes(early),
+            fixed((head_count, LANES)),
             fixed((1, inner_cols)),
             fixed((inner_cols, features)),
             fixed((rows, marked_cols)),
-        ],
+        ]
+        + [pl.BlockSpec(memory_space=pl.ANY)] * 3,
         out_specs=[by_rows(features, late), pl.BlockSpec(memory_space=pl.ANY)],
         out_shape=[
             jax.ShapeDtypeStruct((tok_rows, features), narrow),
             jax.ShapeDtypeStruct((devices * rows, marked_cols), narrow),
         ],
         scratch_shapes=[
+            pltpu.VMEM((blocks, SPAN, head_count), jnp.float32),
+            pltpu.VMEM((blocks, SPAN, head_count), jnp.float32),
+            pltpu.VMEM((blocks, head_count, SPAN), jnp.float32),
+            pltpu.VMEM((blocks, 1, head_count), jnp.float32),
+            pltpu.VMEM((1, head_count), jnp.float32),
+            pltpu.VMEM((1, head_count), jnp.float32),
+            pltpu.VMEM((1, inner_cols), jnp.float32),
+            pltpu.VMEM((2 * RIM, inner_cols), narrow),
+            pltpu.VMEM((2 * RIM, state_cols), narrow),
+            pltpu.VMEM((2 * RIM, state_cols), narrow),
+            dma((3,)), dma((3,)),
             pltpu.VMEM((SPAN + RIM, inner_cols), jnp.float32),
             pltpu.VMEM((SPAN + RIM, state_cols), jnp.float32),
             pltpu.VMEM((SPAN + RIM, state_cols), jnp.float32),
@@ -363,8 +399,8 @@
         ),
         name="mixer_gather",
     )(
-        *x_args, *b_args, *c_args, gating, key_log, cumulative, row_log, end_factor, own_decay,
-        skip, scale, exit_projection, marked,
+        streams[0], filters[0], streams[1], filters[1], streams[2], filters[2], gating, raw, spikes,
+        heads, scale, exit_projection, marked, *streams,
     )
 
 
@@ -441,25 +477,27 @@
     return combined.astype(jnp.bfloat16)
 
 
-def routing_kernel(experts, x_ref, scale_ref, chosen_ref, score_ref, out_ref):
+def routing_kernel(experts, x_ref, scale_ref, chosen_ref, score_ref, out_ref, turned):
     features = x_ref.shape[1]
-    rows, top_count = chosen_ref.shape
+    top_count, rows = chosen_ref.shape
     value = x_ref[...].astype(jnp.float32)
     centred = value - jnp.mean(value, axis=1, keepdims=True)
     spread_of = jnp.mean(centred * centred, axis=1, keepdims=True)
     normed = centred * lax.rsqrt(spread_of + norm_eps) * scale_ref[...]
     out_ref[:, :features] = normed.astype(jnp.bfloat16)
     raised = jnp.exp(score_ref[...])
-    weight = raised / jnp.sum(raised, axis=1, keepdims=True)
+    turned[...] = jnp.zeros_like(turned)
+    turned[0:top_count, :] = chosen_ref[...].astype(jnp.float32)
+    turned[8 : 8 + top_count, :] = raised / jnp.sum(raised, axis=0, keepdims=True)
+    columns = turned[...].T
     lane = lax.broadcasted_iota(jnp.int32, (rows, LANES), 1)
-    named = lax.rem(lane, experts)
-    chosen = chosen_ref[...]
+    named = lax.rem(lane, experts).astype(jnp.float32)
     held = jnp.zeros((rows, LANES), jnp.float32)
     share = jnp.zeros((rows, LANES), jnp.float32)
     for k in range(top_count):
-        same = chosen[:, k : k + 1] == named
+        same = columns[:, k : k + 1] == named
         held = held + jnp.where(same, 1.0, 0.0)
-        share = share + jnp.where(same, weight[:, k : k + 1], 0.0)
+        share = share + jnp.where(same, columns[:, 8 + k : 9 + k], 0.0)
     earlier = lax.broadcasted_iota(jnp.int32, (rows, rows), 0) > lax.broadcasted_iota(
         jnp.int32, (rows, rows), 1
     )
@@ -476,11 +514,11 @@
 
 def experts_kernel(
     experts, capacity, tokens_ref, mix_ref, gate_ref, up_ref, down_ref, out_ref, mixed_ref,
-    tokens, slots, own, outgoing, incoming, place, place_next, from_x, from_y,
-    to_y, came_y, to_x, came_x, keep_a, keep_b, to_z, from_z,
+    tokens, slots, own_a, own_b, outgoing_a, outgoing_b, incoming_a, incoming_b, place, place_next,
+    from_x, from_y, to_y, came_y, to_x, came_x, keep_a, keep_b, to_za, from_za, to_zb, from_zb,
     mix_own, mix_core, mix_out, mix_in, mix_sem, mc_send, mc_recv, mx_send, mx_recv,
     token_sem, core_send, core_recv, x_send, x_recv, y_send, y_recv,
-    a_send, a_recv, b_send, b_recv, z_send, z_recv,
+    a_send, a_recv, b_send, b_recv, za_send, za_recv, zb_send, zb_recv,
 ):
     depth = experts // 2
     steps = experts
@@ -492,14 +530,20 @@
     y_next = {"ep": next_ep}
     rows = out_ref.shape[0]
     features = out_ref.shape[1]
-    half = features // 2
+    cut = own_a.shape[3]
+    own, outgoing, incoming = (own_a, own_b), (outgoing_a, outgoing_b), (incoming_a, incoming_b)
     mesh_id = pl.DeviceIdType.MESH
 
     def z_next(k):
         return {"ep": ((z + k) % depth) * 2 + y}
 
+    def turn(i):
+        middle = depth // 2
+        others = jnp.where(i == 0, middle, jnp.where(i < middle, i, i + 1))
+        return jnp.where(i == depth - 1, 0, others)
+
     def fetch(s):
-        k, dy = (s // 2 + 1) % depth, 1 - s % 2
+        k, dy = turn(s // 2), 1 - s % 2
         block = ((z + k) % depth) * 2 + (y + dy) % 2
         span = 4 * rows
         return pltpu.make_async_copy(
@@ -514,23 +558,27 @@
             device_id=device, device_id_type=mesh_id,
         )
 
-    def core_copy(s):
-        return remote(outgoing.at[s], incoming.at[s], core_send.at[s], core_recv.at[s], sibling)
+    def core_copy(s, side):
+        send, recv = core_send.at[2 * s + side], core_recv.at[2 * s + side]
+        return remote(outgoing[side].at[s], incoming[side].at[s], send, recv, sibling)
 
     def x_copy(s):
-        return remote(own.at[s, 0, 1], from_x.at[s], x_send.at[s], x_recv.at[s], x_next)
+        return remote(own_a.at[s, 1], from_x.at[s], x_send.at[s], x_recv.at[s], x_next)
 
     def y_copy(i):
-        return remote(own.at[2 * i, 1], from_y.at[i], y_send.at[i], y_recv.at[i], y_next)
+        return remote(own_b.at[2 * i], from_y.at[i], y_send.at[i], y_recv.at[i], y_next)
 
     def a_copy(i):
         return remote(to_y.at[i], came_y.at[i], a_send.at[i], a_recv.at[i], y_next)
 
-    def b_copy(i):
-        return remote(to_x.at[i], came_x.at[i], b_send.at[i], b_recv.at[i], x_next)
-
-    def z_copy(i):
-        return remote(to_z.at[i], from_z.at[i], z_send.at[i], z_recv.at[i], z_next(i + 1))
+    def b_copy():
+        return remote(to_x, came_x, b_send.at[0], b_recv.at[0], x_next)
+
+    def za_copy(i):
+        return remote(to_za.at[i], from_za.at[i], za_send.at[i], za_recv.at[i], z_next(turn(i)))
+
+    def zb_copy(i):
+        return remote(to_zb.at[i], from_zb.at[i], zb_send.at[i], zb_recv.at[i], z_next(turn(i)))
 
     chunks, piece = mixed_ref.shape[0] // MIX_ROWS, MIX_ROWS
     share = mixed_ref.shape[0]
@@ -630,7 +678,7 @@
             * (jnp.clip(up_h, -clamp_top, clamp_top) + 1.0)
         ).astype(jnp.bfloat16)
         for side in (0, 1):
-            columns = slice(side * half, (side + 1) * half)
+            columns = slice(0, cut) if side == 0 else slice(cut, features)
             part = jnp.dot(act, down_ref[:, columns], preferred_element_type=jnp.float32)
             for dx in (0, 1):
                 for q in (0, 1):
@@ -639,9 +687,9 @@
                         jnp.bfloat16
                     )
                     if q == 0:
-                        own[s, side, dx] = scaled
+                        own[side][s, dx] = scaled
                     else:
-                        outgoing[s, side, dx] = scaled
+                        outgoing[side][s, dx] = scaled
 
     def spread_out(where, value):
         return jnp.dot(where[:, :capacity], value, preferred_element_type=jnp.float32)
@@ -661,17 +709,18 @@
         @pl.when((s >= 1) & (s <= steps))
         def _():
             t = s - 1
-            core_copy(t).wait_recv()
             for side in (0, 1):
+                core_copy(t, side).wait_recv()
                 for dx in (0, 1):
-                    own[t, side, dx] = (
-                        own[t, side, dx].astype(jnp.float32)
-                        + incoming[t, side, dx].astype(jnp.float32)
+                    own[side][t, dx] = (
+                        own[side][t, dx].astype(jnp.float32)
+                        + incoming[side][t, dx].astype(jnp.float32)
                     ).astype(jnp.bfloat16)
 
         @pl.when(s < steps)
         def _():
-            core_copy(s).start()
+            for side in (0, 1):
+                core_copy(s, side).start()
 
         @pl.when(s == 0)
         def _():
@@ -685,24 +734,34 @@
         @pl.when((s >= 4) & (s % 2 == 0) & (i < depth))
         def _():
             far, near = 2 * i, 2 * i + 1
+            y_copy(i).wait_recv()
+            for dx in (0, 1):
+                sum_b = spread_out(place[near, dx], own_b[near, dx]) + spread_out(
+                    place_next[near, dx], from_y[i, dx]
+                )
+
+                @pl.when(i < depth - 1)
+                def _():
+                    to_zb[i, dx] = sum_b.astype(jnp.bfloat16)
+
+                @pl.when(i == depth - 1)
+                def _():
+                    keep_b[dx] = sum_b
+
             x_copy(far).wait_recv()
             where = place[far, 0]
-            to_y[i] = (spread_out(where, own[far, 0, 0]) + spread_out(where, from_x[far])).astype(
+            to_y[i] = (spread_out(where, own_a[far, 0]) + spread_out(where, from_x[far])).astype(
                 jnp.bfloat16
             )
-            y_copy(i).wait_recv()
-            to_x[i] = (
-                spread_out(place[near, 1], own[near, 1, 1])
-                + spread_out(place_next[near, 1], from_y[i, 1])
-            ).astype(jnp.bfloat16)
+
+            @pl.when(i < depth - 1)
+            def _():
+                zb_copy(i).start()
+
             x_copy(near).wait_recv()
             where = place[near, 0]
-            keep_a[i] = spread_out(where, own[near, 0, 0]) + spread_out(where, from_x[near])
-            keep_b[i] = spread_out(where, own[near, 1, 0]) + spread_out(
-                place_next[near, 0], from_y[i, 0]
-            )
+            keep_a[i] = spread_out(where, own_a[near, 0]) + spread_out(where, from_x[near])
             a_copy(i).start()
-            b_copy(i).start()
 
         @pl.when((s >= 1) & (s <= steps))
         def _():
@@ -728,53 +787,59 @@
         @pl.when((s >= 6) & (s % 2 == 0) & (j < depth))
         def _():
             a_copy(j).wait_recv()
-            b_copy(j).wait_recv()
             sum_a = keep_a[j] + came_y[j].astype(jnp.float32)
-            sum_b = keep_b[j] + came_x[j].astype(jnp.float32)
 
             @pl.when(j < depth - 1)
             def _():
-                to_z[j, :, :half] = sum_a.astype(jnp.bfloat16)
-                to_z[j, :, half:] = sum_b.astype(jnp.bfloat16)
-                z_copy(j).start()
+                to_za[j] = sum_a.astype(jnp.bfloat16)
+                za_copy(j).start()
 
             @pl.when(j == depth - 1)
             def _():
                 keep_a[j] = sum_a
-                keep_b[j] = sum_b
 
         return carry
 
     lax.fori_loop(0, 2 * depth + 5, step, 0)
     for i in range(depth - 1):
-        z_copy(i).wait_recv()
-    for side, keep in ((0, keep_a), (1, keep_b)):
-        columns = slice(side * half, (side + 1) * half)
-        total = keep[depth - 1]
-        for i in range(depth - 1):
-            total = total + from_z[i, :, columns].astype(jnp.float32)
-        out_ref[:, columns] = total.astype(jnp.bfloat16)
+        zb_copy(i).wait_recv()
+    total = [keep_b[0], keep_b[1]]
+    for i in range(depth - 1):
+        total = [total[dx] + from_zb[i, dx].astype(jnp.float32) for dx in (0, 1)]
+    to_x[...] = total[1].astype(jnp.bfloat16)
+    keep_b[0] = total[0]
+    total = keep_a[depth - 1]
+    for i in range(depth - 1):
+        za_copy(i).wait_recv()
+        total = total + from_za[i].astype(jnp.float32)
+    out_ref[:, :cut] = total.astype(jnp.bfloat16)
+    b_copy().start()
     lax.fori_loop(0, chunks, mix_finish, 0)
     lax.fori_loop(0, chunks, mix_sent, 0)
+    b_copy().wait_recv()
+    out_ref[:, cut:] = (keep_b[0] + came_x[...].astype(jnp.float32)).astype(jnp.bfloat16)
     for dx in (0, 1):
         mix_core_copy(dx).wait_send()
     for s in range(steps):
-        core_copy(s).wait_send()
+        for side in (0, 1):
+            core_copy(s, side).wait_send()
         x_copy(s).wait_send()
     for i in range(depth):
         y_copy(i).wait_send()
         a_copy(i).wait_send()
-        b_copy(i).wait_send()
+    b_copy().wait_send()
     for i in range(depth - 1):
-        z_copy(i).wait_send()
+        za_copy(i).wait_send()
+        zb_copy(i).wait_send()
 
 
 def mixer_gather_kernel(
     per_group, groups, blocks, depth,
-    x_ref, xr_ref, xt_ref, b_ref, br_ref, bt_ref, c_ref, cr_ref, ct_ref, z_ref, lw_ref, cum_ref,
-    row_ref, end_ref, decay_ref, skip_ref, scale_ref, exit_ref, marked_ref,
+    x_ref, xt_ref, b_ref, bt_ref, c_ref, ct_ref, z_ref, pre_ref, spike_ref, head_ref, scale_ref,
+    exit_ref, marked_ref, x_all, b_all, c_all,
     part_ref, tokens_ref,
-    xbuf, bbuf, cbuf, state, ybuf, nbuf, pair_out, pair_in, line_out, line_in, line_sum, swap_out,
+    lw_of, cum_of, row_of, end_of, skip_of, decay_of, decay_row, xr_ref, br_ref, cr_ref, rim_s,
+    rim_r, xbuf, bbuf, cbuf, state, ybuf, nbuf, pair_out, pair_in, line_out, line_in, line_sum, swap_out,
     swap_in, local_sem, z_send, z_recv, xa_s, xa_r, xb_s, xb_r, xf_s, xf_r, ya_s, ya_r, yb_s, yb_r,
     yf_s, yf_r, d_s, d_r, pair_s, pair_r, line_s, line_r, swap_s, swap_r,
 ):
@@ -876,22 +941,44 @@
             came(name, k).wait_recv()
             d_sent(k, n).start()
 
+    devices = 2 * depth
+    after, before = {"ep": (ep + 1) % devices}, {"ep": (ep + devices - 1) % devices}
+    last_rows = pl.ds(x_all.shape[0] - 2 * RIM, 2 * RIM)
+
+    def rim_copy(n):
+        whole, rim = ((x_all, xr_ref), (b_all, br_ref), (c_all, cr_ref))[n]
+        return remote(whole.at[last_rows], rim, rim_s.at[n], rim_r.at[n], after)
+
     def own_copy():
         return pltpu.make_async_copy(marked_ref, region(0, 0, 0, None), local_sem.at[0])
 
     @pl.when(step == 0)
     def _():
         barrier = pltpu.get_barrier_semaphore()
-        partners = [sibling, x_next, y_next] + [z_next(k) for k in range(1, depth)]
+        partners = [sibling, x_next, y_next, after, before]
+        partners = partners + [z_next(k) for k in range(1, depth)]
         for partner in partners:
             pl.semaphore_signal(barrier, inc=1, device_id=partner, device_id_type=mesh_id)
         pl.semaphore_wait(barrier, len(partners))
+        for n in range(3):
+            rim_copy(n).start()
         z_copy(1).start()
         first_hop(0)
         for k in range(2, depth - 1):
             z_copy(k).start()
         own_copy().start()
-
+        turned = head_ref[...].T
+        skip_of[...] = turned[2:3]
+        decay_of[...] = jnp.ones_like(decay_of)
+        for n in range(3):
+            rim_copy(n).wait_recv()
+
+    def per_head(row, h):
+        first_head = jnp.broadcast_to(row[:, h : h + 1], (1, 2 * HEAD))
+        second_head = jnp.broadcast_to(row[:, h + 1 : h + 2], (1, 2 * HEAD))
+        return jnp.where(low[0:1], first_head, second_head)
+
+    has_rim = ep > 0
     low = lax.broadcasted_iota(jnp.int32, (SPAN, 2 * HEAD), 1) < HEAD
     state_pass = step < blocks
     output_pass = step > blocks
@@ -899,14 +986,31 @@
     @pl.when(state_pass)
     def _():
         first = step == 0
-        xv = conv_block(xbuf, first, x_ref, xr_ref, xt_ref)
-        bv = conv_block(bbuf, first, b_ref, br_ref, bt_ref)
+        xv = conv_after(xbuf, first, x_ref, xr_ref, has_rim, xt_ref)
+        bv = conv_after(bbuf, first, b_ref, br_ref, has_rim, bt_ref)
 
         @pl.when(first)
         def _():
             state[...] = jnp.zeros_like(state)
 
-        lw = lw_ref[...]
+        raw = pre_ref[...].astype(jnp.float32) + head_ref[:, 0:1]
+        interval = jnp.maximum(raw, 0.0) + jnp.log1p(jnp.exp(-jnp.abs(raw)))
+        fading = spike_ref[...] - jnp.exp(head_ref[:, 1:2]) * interval
+        upto = lax.broadcasted_iota(jnp.int32, (SPAN, SPAN), 0) <= lax.broadcasted_iota(
+            jnp.int32, (SPAN, SPAN), 1
+        )
+        cumulative = jnp.dot(
+            fading, jnp.where(upto, 1.0, 0.0), precision=highest, preferred_element_type=jnp.float32
+        )
+        row_log = jnp.log(interval) - cumulative
+        lw = (row_log + cumulative[:, SPAN - 1 :]).T
+        cum = cumulative.T
+        end = jnp.exp(cum[SPAN - 1 :])
+        row_of[step] = row_log
+        lw_of[step] = lw
+        cum_of[step] = cum
+        end_of[step] = end
+        decay_of[...] = decay_of[...] * end
         for g in range(groups):
             bt = bv[:, g * STATE : (g + 1) * STATE].T.astype(jnp.bfloat16)
             for pair in range(per_group // 2):
@@ -917,7 +1021,7 @@
                 )
                 xw = (xv[:, cols] * factor).astype(jnp.bfloat16)
                 added = jnp.dot(bt, xw, preferred_element_type=jnp.float32)
-                state[:, cols] = state[:, cols] * end_ref[0, :, cols] + added
+                state[:, cols] = state[:, cols] * per_head(end, h) + added
 
     @pl.when(step == blocks // 2)
     def _():
@@ -933,7 +1037,9 @@
                 line_out, line_in.at[k - 1], line_s.at[k - 1], line_r.at[k - 1], z_next(k)
             )
 
-        decay = decay_ref[...]
+        for h in range(0, groups * per_group, 2):
+            decay_row[:, h * HEAD : (h + 2) * HEAD] = per_head(decay_of[...], h)
+        decay = decay_row[...]
         pair_out[:STATE, :] = state[...].astype(jnp.bfloat16)
         pair_out[STATE:, :] = jnp.broadcast_to(decay, (2 * RIM, inner)).astype(jnp.bfloat16)
         last_hop(0, (("xb", 2), ("ya", 4)))
@@ -943,7 +1049,7 @@
         pair.wait_recv()
         mine = pl.ds(pl.multiple_of(y * wide, wide), wide)
         theirs = pl.ds(pl.multiple_of((1 - y) * wide, wide), wide)
-        own_state, own_decay = state[:, mine], decay_ref[:, mine]
+        own_state, own_decay = state[:, mine], decay_row[:, mine]
         other_state = pair_in[:STATE, mine].astype(jnp.float32)
         other_decay = pair_in[STATE : STATE + 1, mine].astype(jnp.float32)
         later = y == 1
@@ -992,11 +1098,13 @@
     @pl.when(output_pass)
     def _():
         first = step == blocks + 1
-        xv = conv_block(xbuf, first, x_ref, xr_ref, xt_ref)
-        bv = conv_block(bbuf, first, b_ref, br_ref, bt_ref)
-        cv = conv_block(cbuf, first, c_ref, cr_ref, ct_ref)
-        lw = lw_ref[...]
-        cum = cum_ref[...]
+        xv = conv_after(xbuf, first, x_ref, xr_ref, has_rim, xt_ref)
+        bv = conv_after(bbuf, first, b_ref, br_ref, has_rim, bt_ref)
+        cv = conv_after(cbuf, first, c_ref, cr_ref, has_rim, ct_ref)
+        at = step - blocks - 1
+        lw = lw_of[at]
+        cum = cum_of[at]
+        end = end_of[at]
         causal = lax.broadcasted_iota(jnp.int32, (SPAN, SPAN), 0) >= lax.broadcasted_iota(
             jnp.int32, (SPAN, SPAN), 1
         )
@@ -1011,7 +1119,7 @@
                 cols = slice(h * HEAD, (h + 2) * HEAD)
                 xp = xv[:, cols]
                 cum_0, cum_1 = spread(cum, h, SPAN), spread(cum, h + 1, SPAN)
-                row_0, row_1 = row_ref[0, h : h + 1, :], row_ref[0, h + 1 : h + 2, :]
+                row_0, row_1 = row_of[at, h : h + 1, :], row_of[at, h + 1 : h + 2, :]
                 m_0 = scores * jnp.exp(jnp.where(causal, cum_0 + row_0, -jnp.inf))
                 m_1 = scores * jnp.exp(jnp.where(causal, cum_1 + row_1, -jnp.inf))
                 mixing = jnp.concatenate([m_0.astype(jnp.bfloat16), m_1.astype(jnp.bfloat16)], axis=1)
@@ -1022,13 +1130,13 @@
                 )
                 before = state[:, cols]
                 carried = jnp.dot(cg, before.astype(jnp.bfloat16), preferred_element_type=jnp.float32)
-                value = value + carried * jnp.exp(jnp.where(low, cum_0, cum_1)) + xp * skip_ref[:, cols]
+                value = value + carried * jnp.exp(jnp.where(low, cum_0, cum_1)) + xp * per_head(skip_of[...], h)
                 factor = jnp.exp(
                     jnp.where(low, spread(lw, h, 2 * HEAD), spread(lw, h + 1, 2 * HEAD))
                 )
                 xw = (xp * factor).astype(jnp.bfloat16)
                 added = jnp.dot(bt, xw, preferred_element_type=jnp.float32)
-                state[:, cols] = before * end_ref[0, :, cols] + added
+                state[:, cols] = before * per_head(end, h) + added
                 gate = z_ref[:, cols].astype(jnp.float32)
                 gated = value * (gate * jax.nn.sigmoid(gate))
                 squares = squares + gated * gated
@@ -1061,6 +1169,8 @@
             for n in range(len(shared)):
                 d_came(k, n).wait_recv()
         own_copy().wait()
+        for n in range(3):
+            rim_copy(n).wait_send()
         for k in range(1, depth):
             z_copy(k).wait_send()
         for k in range(depth):
@@ -1073,7 +1183,7 @@
 def dense_experts_fit(tok_rows, top_count, capacity, mix_rows):
     experts = lax.axis_size("ep")
     fits = experts % 2 == 0 and experts >= 4 and 3 * experts <= LANES and lax.axis_size("tp") == 4
-    return fits and 2 * top_count >= experts and mix_rows % (4 * MIX_ROWS) == 0 and tok_rows == LANES and capacity % 16 == 0
+    return fits and 2 * top_count >= experts and mix_rows % (4 * MIX_ROWS) == 0 and tok_rows == LANES and capacity % 16 == 0 and top_count <= 8
 
 
 def marked_tokens(
@@ -1083,10 +1193,11 @@
     return pl.pallas_call(
         functools.partial(routing_kernel, lax.axis_size("ep")),
         out_shape=jax.ShapeDtypeStruct((rows, features + LANES), jnp.bfloat16),
+        scratch_shapes=[pltpu.VMEM((LANES, rows), jnp.float32)],
         name="routing",
     )(
-        specialist_sample_slice, specialist_scaling_vector[None], chosen_specialists,
-        dispatcher_affinity_matrix,
+        specialist_sample_slice, specialist_scaling_vector[None], chosen_specialists.T,
+        dispatcher_affinity_matrix.T,
     )
 
 
@@ -1095,7 +1206,9 @@
 ):
     experts = lax.axis_size("ep")
     features = gating_projection.shape[1]
-    half, depth, steps = features // 2, experts // 2, experts
+    depth, steps = experts // 2, experts
+    cut = features * CUT_EIGHTHS // 8 // LANES * LANES
+    rest = features - cut
     hidden = gating_projection.shape[2]
     narrow = jnp.bfloat16
     dma = pltpu.SemaphoreType.DMA
@@ -1114,29 +1227,34 @@
         scratch_shapes=[
             pltpu.VMEM((2, 4 * rows, features + LANES), narrow),
             pltpu.VMEM((4 * capacity, features), narrow),
-            pltpu.VMEM((steps, 2, 2, capacity, half), narrow),
-            pltpu.VMEM((steps, 2, 2, capacity, half), narrow),
-            pltpu.VMEM((steps, 2, 2, capacity, half), narrow),
+            pltpu.VMEM((steps, 2, capacity, cut), narrow),
+            pltpu.VMEM((steps, 2, capacity, rest), narrow),
+            pltpu.VMEM((steps, 2, capacity, cut), narrow),
+            pltpu.VMEM((steps, 2, capacity, rest), narrow),
+            pltpu.VMEM((steps, 2, capacity, cut), narrow),
+            pltpu.VMEM((steps, 2, capacity, rest), narrow),
             pltpu.VMEM((steps, 2, rows, LANES), narrow),
             pltpu.VMEM((steps, 2, rows, LANES), narrow),
-            pltpu.VMEM((steps, capacity, half), narrow),
-            pltpu.VMEM((depth, 2, capacity, half), narrow),
-            pltpu.VMEM((depth, rows, half), narrow),
-            pltpu.VMEM((depth, rows, half), narrow),
-            pltpu.VMEM((depth, rows, half), narrow),
-            pltpu.VMEM((depth, rows, half), narrow),
-            pltpu.VMEM((depth, rows, half), jnp.float32),
-            pltpu.VMEM((depth, rows, half), jnp.float32),
-            pltpu.VMEM((depth - 1, rows, features), narrow),
-            pltpu.VMEM((depth - 1, rows, features), narrow),
+            pltpu.VMEM((steps, capacity, cut), narrow),
+            pltpu.VMEM((depth, 2, capacity, rest), narrow),
+            pltpu.VMEM((depth, rows, cut), narrow),
+            pltpu.VMEM((depth, rows, cut), narrow),
+            pltpu.VMEM((rows, rest), narrow),
+            pltpu.VMEM((rows, rest), narrow),
+            pltpu.VMEM((depth, rows, cut), jnp.float32),
+            pltpu.VMEM((2, rows, rest), jnp.float32),
+            pltpu.VMEM((depth - 1, rows, cut), narrow),
+            pltpu.VMEM((depth - 1, rows, cut), narrow),
+            pltpu.VMEM((depth - 1, 2, rows, rest), narrow),
+            pltpu.VMEM((depth - 1, 2, rows, rest), narrow),
             pltpu.VMEM((2, share, features), narrow),
             pltpu.VMEM((2, share, features), narrow),
             pltpu.VMEM((share, features), narrow),
             pltpu.VMEM((share, features), narrow),
             dma((2,)), dma((2,)), dma((2,)), dma((pieces,)), dma((pieces,)),
-            dma((2,)), dma((steps,)), dma((steps,)), dma((steps,)), dma((steps,)),
-            dma((depth,)), dma((depth,)), dma((depth,)), dma((depth,)), dma((depth,)),
-            dma((depth,)), dma((depth - 1,)), dma((depth - 1,)),
+            dma((2,)), dma((2 * steps,)), dma((2 * steps,)), dma((steps,)), dma((steps,)),
+            dma((depth,)), dma((depth,)), dma((depth,)), dma((depth,)), dma((1,)), dma((1,)),
+            dma((depth - 1,)), dma((depth - 1,)), dma((depth - 1,)), dma((depth - 1,)),
         ],
         compiler_params=pltpu.CompilerParams(
             collective_id=0, has_side_effects=True, vmem_limit_bytes=63 * 1024 * 1024

time: 254 us -> 234 us (0.921); the launches traced: 253 us -> 231 us
  local copies, waits for them, and re-layouts: 15.6 us -> 4.27 us
  Pallas kernels: 230 us -> 225 us
  starting transfers between devices: 4.89 us -> 0 us
    pallas_call x1, Pallas kernels: 126 us -> 112 us  [experts_dense(): pl.pallas_call(functools.partial(experts_kernel, experts, capacity), in_s...]
    pallas_call x1, Pallas kernels: 101 us -> 111 us  [mixer_gather(): pl.pallas_call(functools.partial(mixer_gather_kernel, per_group, groups,...]
    ppermute x1 -> x0, starting transfers between devices: 4.89 us -> none  [passed_along(): return lax.ppermute(block, axis, route)]
    slice x5 -> x0, local copies, waits for them, and re-layouts: 3.29 us -> none  [the longest x1 0.72 us: mixer_half(): sequence_entry_features[tok_rows - RIM:]]
    unnamed x6 -> x4, local copies, waits for them, and re-layouts: 6.39 us -> 3.58 us
  transfers between devices with their start and end apart: 1 -> 0, of which waited for: 0 -> 0; matrix products, arithmetic and copies ran while one was open for 4% -> 0% of each run, Pallas kernels for 1% -> 0%
where the time goes in v4:
time: 234 us; the launch traced here: 231 us
  Pallas kernels  225 us (96%)
  local copies, waits for them, and re-layouts  4.27 us (2%)
    pallas_call x1, Pallas kernels, experts_dense(): pl.pallas_call(functools.partial(experts_kernel, experts, capacity), in_s...  112 us
    pallas_call x1, Pallas kernels, mixer_gather(): pl.pallas_call(functools.partial(mixer_gather_kernel, per_group, groups,...  111 us

profile of v4, /device:TPU:0, one launch (start us, length us, event | category | flops | bytes accessed | tf_op | source)
XLA Modules:
  0.0 230.8 jit_solution(4364050680487381717)
XLA Ops:
  0.6 0.7 pad_maximum_fusion
  1.3 0.1 copy.26
  1.4 0.6 pad.4.head_ref
  2.0 2.5 %routing.1.marked_ref = bf16[128,2176]{1,0:T(8,128)(2,1)} custom-call(bf16[128,2048]{1,0:T(8,128)(2,1)} %x_ref.2, f32[1,2048]{1,0:T(1,128)} %bitcast.12, s32[4,128]{1,0:T(4,128)} %bitcast.13, f32[4,128]{1,0:T(4,128)} %bitcast.14), custom_call_target="tpu_custom_call" | custom-call | tf_op jit(solution)/shard_map/routing/pallas_call | solution.py:1193
  4.5 111.2 %mixer_gather.1 = (bf16[1536,2048]{1,0:T(8,128)(2,1)}, bf16[4096,2176]{1,0:T(8,128)(2,1)}) custom-call(bf16[1536,1024]{1,0:T(8,128)(2,1)} %x_all.1, bf16[4,1024]{1,0:T(4,128)(2,1)} %xt_ref.1, bf16[1536,256]{1,0:T(8,128)(2,1)} %b_all.1, bf16[4,256]{1,0:T(4,128)(2,1)} %bt_ref.1, bf16[1536,256]{1,0:T(8,128)(2,1)} %c_all.1, bf16[4,256]{1,0:T(4,128)(2,1)} %ct_ref.1, ...), custom_call_target="tpu_custom_call" | custom-call | flops 9663676416 | bytes 25165824 | tf_op jit(solution)/shard_map/mixer_gather/pallas_call | solution.py:340
  115.7 111.5 %experts.1 = (bf16[128,2048]{1,0:T(8,128)(2,1)}, bf16[384,2048]{1,0:T(8,128)(2,1)}) custom-call(bf16[4096,2176]{1,0:T(8,128)(2,1)} %get-tuple-element.6.tokens_ref, bf16[1536,2048]{1,0:T(8,128)(2,1)} %get-tuple-element.7.mix_ref, bf16[2048,512]{1,0:T(8,128)(2,1)} %bitcast.18, bf16[2048,512]{1,0:T(8,128)(2,1)} %bitcast.19, bf16[512,2048]{1,0:T(8,128)(2,1)} %bitcast.20), custom_call_target="tpu_custom_call" | custom-call | flops 128849018880 | bytes 35651584 | tf_op jit(solution)/shard_map/experts/pallas_call | solution.py:1218
  227.2 0.0 copy-start
  227.2 2.8 %copy.29 = bf16[384,2048]{1,0:T(8,128)(2,1)} copy(bf16[384,2048]{1,0:T(8,128)(2,1)} %get-tuple-element.12) | data formatting | bytes 3145728
  230.0 0.0 copy-done
  230.0 0.8 copy.30
Async XLA Ops:
  227.2 2.8 %copy-start = (bf16[128,2048]{1,0:T(8,128)(2,1)S(1)}, bf16[128,2048]{1,0:T(8,128)(2,1)}, u32[]{:S(2)}) copy-start(bf16[128,2048]{1,0:T(8,128)(2,1)} %get-tuple-element.13) | copy-start | bytes 1572868

commit v5 on v4

--- a/solution.py
+++ b/solution.py
@@ -323,12 +323,6 @@
     def by_rows(width, at):
         return pl.BlockSpec((SPAN, width), lambda i: (at(i), 0))
 
-    def by_lanes(at):
-        return pl.BlockSpec((head_count, SPAN), lambda i: (0, at(i)))
-
-    def early(i):
-        return jnp.minimum(i, blocks - 1)
-
     def fixed(shape):
         return pl.BlockSpec(shape, lambda i: (0, 0))
 
@@ -345,8 +339,8 @@
         + conv_specs(state_cols, late)
         + [
             by_rows(inner_cols, late),
-            by_lanes(early),
-            by_lanes(early),
+            fixed((head_count, tok_rows)),
+            fixed((head_count, tok_rows)),
             fixed((head_count, LANES)),
             fixed((1, inner_cols)),
             fixed((inner_cols, features)),
@@ -583,17 +577,21 @@
     chunks, piece = mixed_ref.shape[0] // MIX_ROWS, MIX_ROWS
     share = mixed_ref.shape[0]
 
-    def mix_rows(dx, c):
+    early, late = chunks // 4, chunks // 2
+
+    def mix_part(n, c):
+        dx, start, stop = ((0, 0, share), (1, early * piece, share), (1, 0, early * piece))[n]
         block = ((x + dx) % 2) * 2 + c
-        return mix_ref.at[pl.ds(pl.multiple_of(block * share, share), share)]
-
-    def mix_fetch(dx):
-        return pltpu.make_async_copy(mix_rows(dx, core), mix_own.at[dx], mix_sem.at[dx])
-
-    def mix_core_copy(dx):
-        return remote(
-            mix_rows(dx, 1 - core), mix_core.at[dx], mc_send.at[dx], mc_recv.at[dx], sibling
-        )
+        rows_n = pl.ds(pl.multiple_of(block * share + start, piece), stop - start)
+        return dx, pl.ds(start, stop - start), mix_ref.at[rows_n]
+
+    def mix_fetch(n):
+        dx, there, source = mix_part(n, core)
+        return pltpu.make_async_copy(source, mix_own.at[dx, there], mix_sem.at[n])
+
+    def mix_core_copy(n):
+        dx, there, source = mix_part(n, 1 - core)
+        return remote(source, mix_core.at[dx, there], mc_send.at[n], mc_recv.at[n], sibling)
 
     def mix_x_copy(j):
         rows_j = pl.ds(pl.multiple_of(j * piece, piece), piece)
@@ -601,11 +599,15 @@
             mix_out.at[rows_j], mix_in.at[rows_j], mx_send.at[j], mx_recv.at[j], x_next
         )
 
-    def mix_piece(j, carry):
+    def mix_away(j, carry):
         rows_j = pl.ds(pl.multiple_of(j * piece, piece), piece)
         mix_out[rows_j, :] = (
             mix_own[1, rows_j, :].astype(jnp.float32) + mix_core[1, rows_j, :].astype(jnp.float32)
         ).astype(jnp.bfloat16)
+        return carry
+
+    def mix_home(j, carry):
+        rows_j = pl.ds(pl.multiple_of(j * piece, piece), piece)
         mix_own[0, rows_j, :] = (
             mix_own[0, rows_j, :].astype(jnp.float32) + mix_core[0, rows_j, :].astype(jnp.float32)
         ).astype(jnp.bfloat16)
@@ -628,16 +630,16 @@
         return carry
 
     fetch(0).start()
-    for dx in (1, 0):
-        mix_fetch(dx).start()
+    for n in (2, 1, 0):
+        mix_fetch(n).start()
     barrier = pltpu.get_barrier_semaphore()
     partners = [sibling, x_next, y_next] + [z_next(k) for k in range(1, depth)]
     for partner in partners:
         pl.semaphore_signal(barrier, inc=1, device_id=partner, device_id_type=mesh_id)
     pl.semaphore_wait(barrier, len(partners))
 
-    for dx in (1, 0):
-        mix_core_copy(dx).start()
+    for n in (2, 1, 0):
+        mix_core_copy(n).start()
 
     lane = lax.broadcasted_iota(jnp.int32, (rows, LANES), 1)
     lane_value = lane.astype(jnp.float32)
@@ -695,6 +697,10 @@
         return jnp.dot(where[:, :capacity], value, preferred_element_type=jnp.float32)
 
     last_x = 2 * depth + 2
+    mix_fetch(2).wait()
+    mix_core_copy(2).wait_recv()
+    lax.fori_loop(0, early, mix_away, 0)
+    lax.fori_loop(0, early, mix_send, 0)
 
     def step(s, carry):
         @pl.when(s < steps)
@@ -722,12 +728,13 @@
             for side in (0, 1):
                 core_copy(s, side).start()
 
-        @pl.when(s == 0)
+        @pl.when(s == 1)
         def _():
-            for dx in (1, 0):
-                mix_fetch(dx).wait()
-                mix_core_copy(dx).wait_recv()
-            lax.fori_loop(0, chunks, mix_piece, 0)
+            for n in (1, 0):
+                mix_fetch(n).wait()
+                mix_core_copy(n).wait_recv()
+            lax.fori_loop(early, chunks, mix_away, 0)
+            lax.fori_loop(0, chunks, mix_home, 0)
 
         i = (s - 4) // 2
 
@@ -772,15 +779,11 @@
             def _():
                 y_copy(t // 2).start()
 
-        early, late = chunks // 4, chunks // 2
-        begin = jnp.where(s == 0, 0, jnp.where(s < last_x, early + s - 3, late))
-        end = jnp.where(s == 0, early, jnp.where(s < last_x, early + s - 2, chunks))
-        lax.fori_loop(
-            jnp.where((s == 0) | (s == last_x), begin, jnp.clip(begin, early, late)),
-            jnp.where((s == 0) | (s == last_x), end,
-                      jnp.where(s > last_x, 0, jnp.clip(end, early, late))),
-            mix_send, 0,
-        )
+        start = jnp.where(s == last_x, late, jnp.clip(early + s - 3, early, late))
+        stop = jnp.where(
+            s == last_x, chunks, jnp.where(s > last_x, 0, jnp.clip(early + s - 2, early, late))
+        )
+        lax.fori_loop(start, stop, mix_send, 0)
 
         j = (s - 6) // 2
 
@@ -818,8 +821,8 @@
     lax.fori_loop(0, chunks, mix_sent, 0)
     b_copy().wait_recv()
     out_ref[:, cut:] = (keep_b[0] + came_x[...].astype(jnp.float32)).astype(jnp.bfloat16)
-    for dx in (0, 1):
-        mix_core_copy(dx).wait_send()
+    for n in range(3):
+        mix_core_copy(n).wait_send()
     for s in range(steps):
         for side in (0, 1):
             core_copy(s, side).wait_send()
@@ -851,7 +854,7 @@
     y_next = {"ep": z * 2 + 1 - y}
     mesh_id = pl.DeviceIdType.MESH
     rows = marked_ref.shape[0]
-    part_rows = rows // 2
+    first_rows = rows * 3 // 8
     inner = state.shape[1]
     wide = inner // 2
 
@@ -866,15 +869,18 @@
 
     def region(dx, dy, k, half, c=core):
         block = (((z + depth - k) % depth) * 2 + (y + dy) % 2) * 4 + ((x + dx) % 2) * 2 + c
-        size = rows if half is None else part_rows
-        start = block * rows + (0 if half is None else half * part_rows)
-        return tokens_ref.at[pl.ds(pl.multiple_of(start, part_rows), size)]
+        offset, size = ((0, rows), (0, first_rows), (first_rows, rows - first_rows))[
+            0 if half is None else 1 + half
+        ]
+        return tokens_ref.at[pl.ds(pl.multiple_of(block * rows + offset, 16), size)]
 
     def source(dx, dy, k, half):
         if (dx, dy, k) == (0, 0, 0):
             if half is None:
                 return marked_ref
-            return marked_ref.at[pl.ds(half * part_rows, part_rows)]
+            if half == 0:
+                return marked_ref.at[pl.ds(0, first_rows)]
+            return marked_ref.at[pl.ds(first_rows, rows - first_rows)]
         return region(dx, dy, k, half)
 
     def z_copy(k):
@@ -969,7 +975,38 @@
         own_copy().start()
         turned = head_ref[...].T
         skip_of[...] = turned[2:3]
-        decay_of[...] = jnp.ones_like(decay_of)
+        heads = head_ref.shape[0]
+
+        def stacked(piece):
+            return jnp.concatenate([piece(n) for n in range(blocks)], axis=0)
+
+        def tall(column):
+            return stacked(lambda n: jnp.broadcast_to(column, (heads, SPAN)))
+
+        raw = stacked(lambda n: pre_ref[:, n * SPAN : (n + 1) * SPAN].astype(jnp.float32))
+        raw = raw + tall(head_ref[:, 0:1])
+        interval = jnp.maximum(raw, 0.0) + jnp.log1p(jnp.exp(-jnp.abs(raw)))
+        spikes = stacked(lambda n: spike_ref[:, n * SPAN : (n + 1) * SPAN])
+        fading = spikes - tall(jnp.exp(head_ref[:, 1:2])) * interval
+        upto = lax.broadcasted_iota(jnp.int32, (SPAN, SPAN), 0) <= lax.broadcasted_iota(
+            jnp.int32, (SPAN, SPAN), 1
+        )
+        cumulative = jnp.dot(
+            fading, jnp.where(upto, 1.0, 0.0), precision=highest, preferred_element_type=jnp.float32
+        )
+        row_log = jnp.log(interval) - cumulative
+        key_log = row_log + cumulative[:, SPAN - 1 :]
+        decay = jnp.ones((1, heads), jnp.float32)
+        for n in range(blocks):
+            rows_n = slice(n * heads, (n + 1) * heads)
+            cum = cumulative[rows_n].T
+            end = jnp.exp(cum[SPAN - 1 :])
+            row_of[n] = row_log[rows_n]
+            lw_of[n] = key_log[rows_n].T
+            cum_of[n] = cum
+            end_of[n] = end
+            decay = decay * end
+        decay_of[...] = decay
         for n in range(3):
             rim_copy(n).wait_recv()
 
@@ -993,24 +1030,8 @@
         def _():
             state[...] = jnp.zeros_like(state)
 
-        raw = pre_ref[...].astype(jnp.float32) + head_ref[:, 0:1]
-        interval = jnp.maximum(raw, 0.0) + jnp.log1p(jnp.exp(-jnp.abs(raw)))
-        fading = spike_ref[...] - jnp.exp(head_ref[:, 1:2]) * interval
-        upto = lax.broadcasted_iota(jnp.int32, (SPAN, SPAN), 0) <= lax.broadcasted_iota(
-            jnp.int32, (SPAN, SPAN), 1
-        )
-        cumulative = jnp.dot(
-            fading, jnp.where(upto, 1.0, 0.0), precision=highest, preferred_element_type=jnp.float32
-        )
-        row_log = jnp.log(interval) - cumulative
-        lw = (row_log + cumulative[:, SPAN - 1 :]).T
-        cum = cumulative.T
-        end = jnp.exp(cum[SPAN - 1 :])
-        row_of[step] = row_log
-        lw_of[step] = lw
-        cum_of[step] = cum
-        end_of[step] = end
-        decay_of[...] = decay_of[...] * end
+        lw = lw_of[step]
+        end = end_of[step]
         for g in range(groups):
             bt = bv[:, g * STATE : (g + 1) * STATE].T.astype(jnp.bfloat16)
             for pair in range(per_group // 2):
@@ -1151,9 +1172,9 @@
 
     pace = blocks // (2 * depth - 2)
     for k in range(2, depth):
-        at = blocks + 1 + (2 * k - 3) * pace
-
-        @pl.when(step == at)
+        at = blocks + 1 + (2 * k - 4) * pace
+
+        @pl.when(step == at - (1 if k == 2 else 0))
         def _():
             first_hop(k)
 
@@ -1251,7 +1272,7 @@
             pltpu.VMEM((2, share, features), narrow),
             pltpu.VMEM((share, features), narrow),
             pltpu.VMEM((share, features), narrow),
-            dma((2,)), dma((2,)), dma((2,)), dma((pieces,)), dma((pieces,)),
+            dma((3,)), dma((3,)), dma((3,)), dma((pieces,)), dma((pieces,)),
             dma((2,)), dma((2 * steps,)), dma((2 * steps,)), dma((steps,)), dma((steps,)),
             dma((depth,)), dma((depth,)), dma((depth,)), dma((depth,)), dma((1,)), dma((1,)),
             dma((depth - 1,)), dma((depth - 1,)), dma((depth - 1,)), dma((depth - 1,)),

time: 234 us -> 227 us (0.970)
  Pallas kernels: 225 us -> 219 us
    pallas_call x1, Pallas kernels: 111 us -> 101 us  [mixer_gather(): pl.pallas_call(functools.partial(mixer_gather_kernel, per_group, groups,...]
    pallas_call x1, Pallas kernels: 112 us -> 115 us  [experts_dense(): pl.pallas_call(functools.partial(experts_kernel, experts, capacity), in_s...]
where the time goes in v5:
time: 227 us; the launch traced here: 224 us
  Pallas kernels  219 us (96%)
  local copies, waits for them, and re-layouts  4.27 us (2%)
    pallas_call x1, Pallas kernels, experts_dense(): pl.pallas_call(functools.partial(experts_kernel, experts, capacity), in_s...  115 us
    pallas_call x1, Pallas kernels, mixer_gather(): pl.pallas_call(functools.partial(mixer_gather_kernel, per_group, groups,...  101 us

profile of v5, /device:TPU:0, one launch (start us, length us, event | category | flops | bytes accessed | tf_op | source)
XLA Modules:
  0.0 224.4 jit_solution(4677265141676159171)
XLA Ops:
  0.6 0.7 pad_maximum_fusion
  1.3 0.1 copy.26
  1.4 0.6 pad.4.head_ref
  2.0 2.5 %routing.1.marked_ref = bf16[128,2176]{1,0:T(8,128)(2,1)} custom-call(bf16[128,2048]{1,0:T(8,128)(2,1)} %x_ref.2, f32[1,2048]{1,0:T(1,128)} %bitcast.12, s32[4,128]{1,0:T(4,128)} %bitcast.13, f32[4,128]{1,0:T(4,128)} %bitcast.14), custom_call_target="tpu_custom_call" | custom-call | tf_op jit(solution)/shard_map/routing/pallas_call | solution.py:1214
  4.5 100.9 %mixer_gather.1 = (bf16[1536,2048]{1,0:T(8,128)(2,1)}, bf16[4096,2176]{1,0:T(8,128)(2,1)}) custom-call(bf16[1536,1024]{1,0:T(8,128)(2,1)} %x_all.1, bf16[4,1024]{1,0:T(4,128)(2,1)} %xt_ref.1, bf16[1536,256]{1,0:T(8,128)(2,1)} %b_all.1, bf16[4,256]{1,0:T(4,128)(2,1)} %bt_ref.1, bf16[1536,256]{1,0:T(8,128)(2,1)} %c_all.1, bf16[4,256]{1,0:T(4,128)(2,1)} %ct_ref.1, ...), custom_call_target="tpu_custom_call" | custom-call | flops 9663676416 | bytes 25165824 | tf_op jit(solution)/shard_map/mixer_gather/pallas_call | solution.py:334
  105.4 115.5 %experts.1 = (bf16[128,2048]{1,0:T(8,128)(2,1)}, bf16[384,2048]{1,0:T(8,128)(2,1)}) custom-call(bf16[4096,2176]{1,0:T(8,128)(2,1)} %get-tuple-element.6.tokens_ref, bf16[1536,2048]{1,0:T(8,128)(2,1)} %get-tuple-element.7.mix_ref, bf16[2048,512]{1,0:T(8,128)(2,1)} %bitcast.18, bf16[2048,512]{1,0:T(8,128)(2,1)} %bitcast.19, bf16[512,2048]{1,0:T(8,128)(2,1)} %bitcast.20), custom_call_target="tpu_custom_call" | custom-call | flops 128849018880 | bytes 35651584 | tf_op jit(solution)/shard_map/experts/pallas_call | solution.py:1239
  220.8 0.0 copy-start
  220.9 2.8 %copy.29 = bf16[384,2048]{1,0:T(8,128)(2,1)} copy(bf16[384,2048]{1,0:T(8,128)(2,1)} %get-tuple-element.12) | data formatting | bytes 3145728
  223.6 0.0 copy-done
  223.6 0.8 copy.30
Async XLA Ops:
  220.8 2.8 %copy-start = (bf16[128,2048]{1,0:T(8,128)(2,1)S(1)}, bf16[128,2048]{1,0:T(8,128)(2,1)}, u32[]{:S(2)}) copy-start(bf16[128,2048]{1,0:T(8,128)(2,1)} %get-tuple-element.13) | copy-start | bytes 1572868

commit v6 on v5

--- a/solution.py
+++ b/solution.py
@@ -192,13 +192,13 @@
     local_groups = memory_insert_clusters.shape[1] // STATE
     per_group = local_heads // local_groups
     if marked is not None:
-        heads = jnp.stack([interval_offset, head_fading_exponent, skip_connection_factor], axis=1)
         return mixer_gather(
             per_group, local_groups, tok_rows // SPAN,
             (sequence_entry_features, memory_insert_clusters, memory_query_clusters),
             (entry_filter_taps, insert_filter_taps, query_filter_taps), sequence_exit_gating,
             interval_presoftplus.T, spike_fading_exponent.T,
-            jnp.pad(heads, ((0, 0), (0, LANES - heads.shape[1]))), cluster_scaling_vector[None],
+            (interval_offset[None], head_fading_exponent[None], skip_connection_factor[None]),
+            cluster_scaling_vector[None],
             sequence_exit_projection, marked,
         )
     inner_cols = sequence_entry_features.shape[1]
@@ -341,7 +341,9 @@
             by_rows(inner_cols, late),
             fixed((head_count, tok_rows)),
             fixed((head_count, tok_rows)),
-            fixed((head_count, LANES)),
+            fixed((1, head_count)),
+            fixed((1, head_count)),
+            fixed((1, head_count)),
             fixed((1, inner_cols)),
             fixed((inner_cols, features)),
             fixed((rows, marked_cols)),
@@ -353,6 +355,7 @@
             jax.ShapeDtypeStruct((devices * rows, marked_cols), narrow),
         ],
         scratch_shapes=[
+            pltpu.VMEM((LANES, LANES), jnp.float32),
             pltpu.VMEM((blocks, SPAN, head_count), jnp.float32),
             pltpu.VMEM((blocks, SPAN, head_count), jnp.float32),
             pltpu.VMEM((blocks, head_count, SPAN), jnp.float32),
@@ -394,7 +397,7 @@
         name="mixer_gather",
     )(
         streams[0], filters[0], streams[1], filters[1], streams[2], filters[2], gating, raw, spikes,
-        heads, scale, exit_projection, marked, *streams,
+        *heads, scale, exit_projection, marked, *streams,
     )
 
 
@@ -838,10 +841,10 @@
 
 def mixer_gather_kernel(
     per_group, groups, blocks, depth,
-    x_ref, xt_ref, b_ref, bt_ref, c_ref, ct_ref, z_ref, pre_ref, spike_ref, head_ref, scale_ref,
+    x_ref, xt_ref, b_ref, bt_ref, c_ref, ct_ref, z_ref, pre_ref, spike_ref, offset_ref, rate_ref, skip_ref, scale_ref,
     exit_ref, marked_ref, x_all, b_all, c_all,
     part_ref, tokens_ref,
-    lw_of, cum_of, row_of, end_of, skip_of, decay_of, decay_row, xr_ref, br_ref, cr_ref, rim_s,
+    head_rows, lw_of, cum_of, row_of, end_of, skip_of, decay_of, decay_row, xr_ref, br_ref, cr_ref, rim_s,
     rim_r, xbuf, bbuf, cbuf, state, ybuf, nbuf, pair_out, pair_in, line_out, line_in, line_sum, swap_out,
     swap_in, local_sem, z_send, z_recv, xa_s, xa_r, xb_s, xb_r, xf_s, xf_r, ya_s, ya_r, yb_s, yb_r,
     yf_s, yf_r, d_s, d_r, pair_s, pair_r, line_s, line_r, swap_s, swap_r,
@@ -973,9 +976,12 @@
         for k in range(2, depth - 1):
             z_copy(k).start()
         own_copy().start()
-        turned = head_ref[...].T
-        skip_of[...] = turned[2:3]
-        heads = head_ref.shape[0]
+        heads = pre_ref.shape[0]
+        head_rows[...] = jnp.zeros_like(head_rows)
+        head_rows[0:1, 0:heads] = offset_ref[...]
+        head_rows[1:2, 0:heads] = jnp.exp(rate_ref[...])
+        skip_of[...] = skip_ref[...]
+        by_head = head_rows[...].T[0:heads]
 
         def stacked(piece):
             return jnp.concatenate([piece(n) for n in range(blocks)], axis=0)
@@ -984,10 +990,10 @@
             return stacked(lambda n: jnp.broadcast_to(column, (heads, SPAN)))
 
         raw = stacked(lambda n: pre_ref[:, n * SPAN : (n + 1) * SPAN].astype(jnp.float32))
-        raw = raw + tall(head_ref[:, 0:1])
+        raw = raw + tall(by_head[:, 0:1])
         interval = jnp.maximum(raw, 0.0) + jnp.log1p(jnp.exp(-jnp.abs(raw)))
         spikes = stacked(lambda n: spike_ref[:, n * SPAN : (n + 1) * SPAN])
-        fading = spikes - tall(jnp.exp(head_ref[:, 1:2])) * interval
+        fading = spikes - tall(by_head[:, 1:2]) * interval
         upto = lax.broadcasted_iota(jnp.int32, (SPAN, SPAN), 0) <= lax.broadcasted_iota(
             jnp.int32, (SPAN, SPAN), 1
         )

time: 227 us -> 226 us (level)
  no operation moved by 1% of the time
where the time goes in v6:
time: 226 us; the launch traced here: 223 us
  Pallas kernels  219 us (97%)
  local copies, waits for them, and re-layouts  3.58 us (2%)
    pallas_call x1, Pallas kernels, experts_dense(): pl.pallas_call(functools.partial(experts_kernel, experts, capacity), in_s...  115 us
    pallas_call x1, Pallas kernels, mixer_gather(): pl.pallas_call(functools.partial(mixer_gather_kernel, per_group, groups,...  101 us

profile of v6, /device:TPU:0, one launch (start us, length us, event | category | flops | bytes accessed | tf_op | source)
XLA Modules:
  0.0 223.2 jit_solution(13220330585650710118)
XLA Ops:
  0.6 2.5 %routing.1.marked_ref = bf16[128,2176]{1,0:T(8,128)(2,1)} custom-call(bf16[128,2048]{1,0:T(8,128)(2,1)} %x_ref.2, f32[1,2048]{1,0:T(1,128)} %bitcast.12, s32[4,128]{1,0:T(4,128)} %bitcast.13, f32[4,128]{1,0:T(4,128)} %bitcast.14), custom_call_target="tpu_custom_call" | custom-call | tf_op jit(solution)/shard_map/routing/pallas_call | solution.py:1220
  3.1 101.2 %mixer_gather.1 = (bf16[1536,2048]{1,0:T(8,128)(2,1)}, bf16[4096,2176]{1,0:T(8,128)(2,1)}) custom-call(bf16[1536,1024]{1,0:T(8,128)(2,1)} %x_all.1, bf16[4,1024]{1,0:T(4,128)(2,1)} %xt_ref.1, bf16[1536,256]{1,0:T(8,128)(2,1)} %b_all.1, bf16[4,256]{1,0:T(4,128)(2,1)} %bt_ref.1, bf16[1536,256]{1,0:T(8,128)(2,1)} %c_all.1, bf16[4,256]{1,0:T(4,128)(2,1)} %ct_ref.1, ...), custom_call_target="tpu_custom_call" | custom-call | flops 9663676416 | bytes 25165824 | tf_op jit(solution)/shard_map/mixer_gather/pallas_call | solution.py:334
  104.3 115.3 %experts.1 = (bf16[128,2048]{1,0:T(8,128)(2,1)}, bf16[384,2048]{1,0:T(8,128)(2,1)}) custom-call(bf16[4096,2176]{1,0:T(8,128)(2,1)} %get-tuple-element.6.tokens_ref, bf16[1536,2048]{1,0:T(8,128)(2,1)} %get-tuple-element.7.mix_ref, bf16[2048,512]{1,0:T(8,128)(2,1)} %bitcast.15, bf16[2048,512]{1,0:T(8,128)(2,1)} %bitcast.16, bf16[512,2048]{1,0:T(8,128)(2,1)} %bitcast.17), custom_call_target="tpu_custom_call" | custom-call | flops 128849018880 | bytes 35651584 | tf_op jit(solution)/shard_map/experts/pallas_call | solution.py:1245
  219.6 0.0 copy-start
  219.6 2.8 %copy.25 = bf16[384,2048]{1,0:T(8,128)(2,1)} copy(bf16[384,2048]{1,0:T(8,128)(2,1)} %get-tuple-element.12) | data formatting | bytes 3145728
  222.4 0.0 copy-done
  222.4 0.8 copy.26
Async XLA Ops:
  219.6 2.8 %copy-start = (bf16[128,2048]{1,0:T(8,128)(2,1)S(1)}, bf16[128,2048]{1,0:T(8,128)(2,1)}, u32[]{:S(2)}) copy-start(bf16[128,2048]{1,0:T(8,128)(2,1)} %get-tuple-element.13) | copy-start | bytes 1572868
